TPU v7x, 128 devices: a whole 4x4x4 slice. The times are simulated.
128 devices in a mesh: sp: 16 (over z, x), tp: 8 (over y, core).
Axes of the slice: x: 4, y: 4, z: 4, core: 2. Of those that a mesh axis runs over, the one named last changes fastest.
Arguments:
- queries: bfloat16 [16384, 1024], P('sp', 'tp'), may hold values from -75 to 75
- key_rows: bfloat16 [16384, 1024], P('sp', 'tp'), may hold values from -4 to 4
- value_rows: bfloat16 [16384, 1024], P('sp', 'tp'), may hold values from -6 to 6
- cum_gate: float32 [16, 16384], P('tp'), may hold values from -2342 to 0, as said below
- residual: bfloat16 [16384, 2048], P(('sp', 'tp')), may hold values from -6 to 6
- out_weight: bfloat16 [1024, 2048], replicated, may hold values from -0.1875 to 0.1875
- gain_mix: float32 [2048], replicated, may hold values from 0.1 to 1.9
- gain_pre: float32 [2048], replicated, may hold values from 0.1 to 1.9
- gain_post: float32 [2048], replicated, may hold values from 0.1 to 1.9
- route_ids: int32 [16384, 2], P(('sp', 'tp')), may hold values from 0 to 127, all different within a row; in each aligned block of 128 rows (0 to 127, 128 to 255, ...) at most 3 rows name the same one
- route_weight: float32 [16384, 2], P(('sp', 'tp')), may hold values from 0.2 to 1
- w_gate: bfloat16 [128, 2048, 512], P(('sp', 'tp')), may hold values from -0.125 to 0.125
- w_up: bfloat16 [128, 2048, 512], P(('sp', 'tp')), may hold values from -0.125 to 0.125
- w_down: bfloat16 [128, 512, 2048], P(('sp', 'tp')), may hold values from -0.25 to 0.25
Outputs:
- layer_out: bfloat16 [16384, 2048], P(('sp', 'tp'))
Inputs may be any that keep to these rules, and one draw needn't show every extreme that they name: `route_ids`: each row names 2 different experts; in the rows of one device no expert is named more than 3 times, a bound that some block reaches. `cum_gate`: along the positions each head's values never rise.
All inputs are finite; a program needn't handle non-finite values.
Results may differ from a plain program's by a relative error of at most 0.018.
Values may be sent and summed in bfloat16 or wider, within the bound.
No kernel may reach another device: no remote copies, remote signals or barrier semaphores. Data moves between devices by JAX's collectives and lax.ppermute only.
A program may use at most 64 MiB of HBM per device.

v0:
```python
import math

import jax
import jax.numpy as jnp
from jax import lax
from jax.sharding import PartitionSpec as P

HEAD_DIM = 64


NORM_EPS = 1e-06
MASKED = -1e30


def rms_scale(rows, gain):
    mean_sq = jnp.mean(rows * rows, axis=-1, keepdims=True)
    return rows * lax.rsqrt(mean_sq + NORM_EPS) * gain


def attend(running, queries, gate_q, q_start, key_part, value_part, gate_k, k_start):
    row_peak, row_total, weighted = running
    scores = jnp.einsum(
        "qhd,khd->hqk", queries, key_part, preferred_element_type=jnp.float32
    ) * HEAD_DIM ** (-0.5)
    scores = scores + gate_q[:, :, None] - gate_k[:, None, :]
    query_pos = q_start + lax.iota(jnp.int32, queries.shape[0])
    key_pos = k_start + lax.iota(jnp.int32, key_part.shape[0])
    allowed = (key_pos[None, :] <= query_pos[:, None])[None]
    scores = jnp.where(allowed, scores, MASKED)
    new_peak = jnp.maximum(row_peak, jnp.max(scores, axis=-1))
    unnorm = jnp.where(allowed, jnp.exp(scores - new_peak[..., None]), 0.0)
    rescale = jnp.exp(row_peak - new_peak)
    row_total = row_total * rescale + jnp.sum(unnorm, axis=-1)
    weighted = weighted * rescale.T[:, :, None] + jnp.einsum(
        "hqk,khd->qhd", unnorm.astype(jnp.bfloat16), value_part, preferred_element_type=jnp.float32
    )
    return (new_peak, row_total, weighted)


def local(
    queries,
    key_rows,
    value_rows,
    cum_gate,
    residual,
    out_weight,
    gain_mix,
    gain_pre,
    gain_post,
    route_ids,
    route_weight,
    w_gate,
    w_up,
    w_down,
):
    tok_dev, feature_width = queries.shape
    local_heads = feature_width // HEAD_DIM
    my_start = lax.axis_index("sp") * tok_dev
    query_heads = queries.reshape(tok_dev, local_heads, HEAD_DIM)
    gate_q = lax.dynamic_slice_in_dim(cum_gate, my_start, tok_dev, 1)
    initial = (
        jnp.full((local_heads, tok_dev), MASKED, jnp.float32),
        jnp.zeros((local_heads, tok_dev), jnp.float32),
        jnp.zeros((tok_dev, local_heads, HEAD_DIM), jnp.float32),
    )
    paired = jnp.stack((key_rows, value_rows))

    def consume(running, key_part, value_part, k_start):
        row_count = key_part.shape[0]
        gate_k = lax.dynamic_slice_in_dim(cum_gate, k_start, row_count, 1)
        return attend(
            running,
            query_heads,
            gate_q,
            my_start,
            key_part.reshape(row_count, local_heads, HEAD_DIM),
            value_part.reshape(row_count, local_heads, HEAD_DIM),
            gate_k,
            k_start,
        )

    running = initial
    piece = lax.all_gather(paired, "sp", axis=1, tiled=True)
    row_count = piece.shape[1]
    span_rows = math.gcd(row_count, tok_dev)

    def single(block_index, running):
        offset = block_index * span_rows
        part = lax.dynamic_slice_in_dim(piece, offset, span_rows, 1)
        return lax.cond(
            offset < my_start + tok_dev,
            lambda state_now: consume(state_now, part[0], part[1], offset),
            lambda state_now: state_now,
            running,
        )

    running = lax.fori_loop(0, row_count // span_rows, single, running)
    row_peak, row_total, weighted = running
    attended = (
        (weighted / row_total.T[:, :, None]).astype(jnp.bfloat16).reshape(tok_dev, feature_width)
    )
    head_rows = lax.all_to_all(attended, "tp", split_axis=0, concat_axis=1, tiled=True)
    projected = jnp.dot(head_rows, out_weight, preferred_element_type=jnp.float32)
    stream = (residual.astype(jnp.float32) + rms_scale(projected, gain_mix)).astype(jnp.bfloat16)
    stream_wide = lax.optimization_barrier(stream).astype(jnp.float32)
    normed = rms_scale(stream_wide, gain_pre).astype(jnp.bfloat16)
    rows_dev, top_count = route_ids.shape
    model_width = normed.shape[1]
    experts_all = lax.axis_size("sp") * lax.axis_size("tp")
    capacity = max(2, (4 * rows_dev * top_count + 3 * experts_all - 1) // (3 * experts_all))
    flat_ids = route_ids.reshape(-1)
    onehot = (flat_ids[:, None] == lax.iota(jnp.int32, experts_all)[None, :]).astype(jnp.int32)
    slot_rank = jnp.sum(jnp.cumsum(onehot, axis=0) * onehot, axis=1) - 1
    slot_index = flat_ids * capacity + slot_rank
    spread = jnp.repeat(normed, top_count, axis=0)
    outgoing = (
        jnp.zeros((experts_all * capacity, model_width), jnp.bfloat16).at[slot_index].set(spread)
    )
    outgoing = outgoing.reshape(experts_all, capacity, model_width)
    arrived = lax.all_to_all(outgoing, ("sp", "tp"), split_axis=0, concat_axis=0, tiled=True)
    sources, slots, width_here = arrived.shape
    flat_rows = arrived.reshape(sources * slots, width_here)
    gate_act = jnp.dot(flat_rows, w_gate[0], preferred_element_type=jnp.float32)
    up_act = jnp.dot(flat_rows, w_up[0], preferred_element_type=jnp.float32)
    hidden = (jax.nn.silu(gate_act) * up_act).astype(jnp.bfloat16)
    expert_out = jnp.dot(hidden, w_down[0], preferred_element_type=jnp.float32).astype(jnp.bfloat16)
    returned = lax.all_to_all(
        expert_out.reshape(sources, slots, width_here),
        ("sp", "tp"),
        split_axis=0,
        concat_axis=0,
        tiled=True,
    )
    picked = returned.reshape(experts_all * capacity, model_width)[slot_index]
    picked = picked.reshape(rows_dev, top_count, model_width).astype(jnp.float32)
    combined = jnp.sum(picked * route_weight[:, :, None], axis=1)
    return (stream_wide + rms_scale(combined, gain_post)).astype(jnp.bfloat16)


def solution(mesh):
    return jax.shard_map(
        local,
        mesh=mesh,
        in_specs=(
            P("sp", "tp"),
            P("sp", "tp"),
            P("sp", "tp"),
            P("tp", None),
            P(("sp", "tp"), None),
            P(),
            P(),
            P(),
            P(),
            P(("sp", "tp"), None),
            P(("sp", "tp"), None),
            P(("sp", "tp"), None, None),
            P(("sp", "tp"), None, None),
            P(("sp", "tp"), None, None),
        ),
        out_specs=P(("sp", "tp"), None),
        check_vma=False,
    )
```

profile of v0, /device:TPU:1, one launch (start us, length us, event | category | flops | bytes accessed | tf_op | source)
XLA Modules:
  0.0 409.1 jit_solution(8245087762462546506)
XLA Ops:
  6.5 1.2 copy.42
  7.8 1.1 copy.43
  8.9 0.8 pad_maximum_fusion
  9.8 0.8 copy.47
  10.8 1.1 copy.44
  13.2 70.6 %all-gather.2.cloned.1.call-done = bf16[2,16384,128]{1,2,0:T(8,128)(2,1)} async-done(((bf16[2,1024,128]{1,2,0:T(8,128)(2,1)}), bf16[2,16384,128]{1,2,0:T(8,128)(2,1)}) %all-gather.2.cloned.1.call-update) | async-done | bytes 8388624 | tf_op jit(solution)/shard_map/all_gather | solution.py:83
  84.0 11.8 %while.18 = (s32[]{:T(128)}, f32[2,1024]{1,0:T(2,128)S(1)}, f32[2,1024]{1,0:T(2,128)S(1)}, f32[1024,2,64]{0,2,1:T(8,128)S(1)}, s32[]{:T(128)}, /*index=5*/s32[]{...) while((s32[]{:T(128)}, f32[2,1024]{1,0:T(2,128)S(1)}, ...), condition=%wide.region_5.6_spmd, body=%wide.region_0.5_spmd.sunk | while | flops 578035712 | bytes 32457040 | solution.py:97
  84.0 11.1 %conditional.2 = ((f32[2,1024]{1,0:T(2,128)S(1)}, f32[2,1024]{1,0:T(2,128)S(1)}, f32[1024,2,64]{0,2,1:T(8,128)S(1)})) conditional(s32[]{:T(128)} %convert_element_type.89, (f32[2,1024]{1,0:T(2,128)S(1)}, f32[2,1024]{1,0:T(2,128)S(1)}, f32[1024,2,64]{0,2,1:T(8,128)S(1)}) %tuple.52, (s32[]{:T(128)}, s32[]{:T(128)}, bf16[2,16384,128]{1,2,0:T(8,128)(2,1)}, ...), branch_computations={%region_1.0_spmd, %region_2.4_spmd} | conditional | flops 578035712 | bytes 32456802 | solution.py:90
  84.7 1.1 constant_dynamic-slice_fusion.2
  86.4 2.4 fusion.2
  88.9 3.2 fusion.9
  92.1 3.0 fusion.1
  95.9 0.7 copy.45
  96.6 5.1 %all-to-all-start = ((bf16[8,128,128]{1,2,0:T(8,128)(2,1)}), bf16[8,128,128]{1,2,0:T(8,128)(2,1)S(1)}, u32[]{:S(2)}, u32[]{:S(2)}) async-start(bf16[8,128,128]{1,2,0:T(8,128)(2,1)} %copy.45), calls=%async_computation | async-start | bytes 524288 | tf_op jit(solution)/shard_map/all_to_all | solution.py:102
  102.0 6.2 %all-to-all-done = bf16[8,128,128]{1,2,0:T(8,128)(2,1)S(1)} async-done(((bf16[8,128,128]{1,2,0:T(8,128)(2,1)}), bf16[8,128,128]{1,2,0:T(8,128)(2,1)S(1)}, u32[]{:S(2)}, u32[]{:S(2)}) %all-to-all-start) | async-done | bytes 262176 | tf_op jit(solution)/shard_map/all_to_all | solution.py:102
  108.2 3.0 multiply_reduce_fusion.2
  111.9 1.7 broadcast_in_dim.62
  113.6 2.3 reshape.167
  115.8 4.1 %scatter_custom_fusion = bf16[384,2048]{1,0:T(8,128)(2,1)} fusion(s32[256]{0:T(256)S(1)} %bitcast.80, bf16[256,2048]{1,0:T(8,128)(2,1)} %reshape.167, bf16[]{:T(256)} %constant.98.clone.1), kind=kCustom, calls=%fused_computation.47 | custom fusion | bytes 1573376 | tf_op jit(solution)/shard_map/scatter | solution.py:117
  120.0 5.1 %reshape.150 = bf16[128,3,2048]{2,1,0:T(4,128)(2,1)} reshape(bf16[384,2048]{1,0:T(8,128)(2,1)} %scatter_custom_fusion) | data formatting | bytes 3145728 | tf_op jit(solution)/shard_map/reshape | solution.py:119
  125.1 202.5 %all_to_all.29 = bf16[128,3,2048]{2,1,0:T(4,128)(2,1)} all-to-all(bf16[128,3,2048]{2,1,0:T(4,128)(2,1)} %reshape.150), channel_id=1, replica_groups=mesh['sp'=16,'tp'=8] {'sp','tp'}, dimensions={0} | all-to-all | bytes 3145728 | tf_op jit(solution)/shard_map/all_to_all | solution.py:120
  327.6 5.0 %reshape.151 = bf16[384,2048]{1,0:T(8,128)(2,1)} reshape(bf16[128,3,2048]{2,1,0:T(4,128)(2,1)} %all_to_all.29) | data formatting | bytes 3145728 | tf_op jit(solution)/shard_map/reshape | solution.py:122
  332.7 3.9 fusion.19
  336.6 5.3 %convolution_convert_fusion = bf16[384,2048]{1,0:T(8,128)(2,1)} fusion(bf16[1,512,2048]{2,1,0:T(8,128)(2,1)S(1)} %copy-done, bf16[384,2048]{1,0:T(8,128)(2,1)} %reshape.151, bf16[1,2048,512]{2,1,0:T(8,128)(2,1)} %param.30, f32[384,512]{1,0:T(8,128)} %fusion.19), kind=kOutput, calls=%fused_computation.23 | convolution fusion | flops 1612578816 | bytes 8126464 | tf_op jit(solution)/shard_map/dot_general | solution.py:126
  341.9 5.2 %reshape.152 = bf16[128,3,2048]{2,1,0:T(4,128)(2,1)} reshape(bf16[384,2048]{1,0:T(8,128)(2,1)} %convolution_convert_fusion) | data formatting | bytes 3145728 | tf_op jit(solution)/shard_map/reshape | solution.py:128
  347.1 5.8 %all-to-all-start.2 = ((bf16[128,3,2048]{2,1,0:T(4,128)(2,1)}), bf16[128,3,2048]{2,1,0:T(4,128)(2,1)}, u32[]{:S(2)}, u32[]{:S(2)}) async-start(bf16[128,3,2048]{2,1,0:T(4,128)(2,1)} %reshape.152), calls=%async_computation.2 | async-start | bytes 4194304 | tf_op jit(solution)/shard_map/all_to_all | solution.py:127
  353.0 29.7 %all-to-all-done.2 = bf16[128,3,2048]{2,1,0:T(4,128)(2,1)} async-done(((bf16[128,3,2048]{2,1,0:T(4,128)(2,1)}), bf16[128,3,2048]{2,1,0:T(4,128)(2,1)}, u32[]{:S(2)}, u32[]{:S(2)}) %all-to-all-start.2) | async-done | bytes 1572896 | tf_op jit(solution)/shard_map/all_to_all | solution.py:127
  382.8 5.1 %reshape.153 = bf16[384,2048]{1,0:T(8,128)(2,1)} reshape(bf16[128,3,2048]{2,1,0:T(4,128)(2,1)} %all-to-all-done.2) | data formatting | bytes 3145728 | tf_op jit(solution)/shard_map/reshape | solution.py:134
  387.9 4.9 %gather_fusion = bf16[256,2048]{1,0:T(8,128)(2,1)} fusion(bf16[384,2048]{1,0:T(8,128)(2,1)} %reshape.153, s32[1024]{0:T(1024)S(1)} %pad_clamp_fusion), kind=kCustom, calls=%fused_computation | custom fusion | bytes 2098176 | tf_op jit(solution)/shard_map/gather | solution.py:134
  392.8 3.4 reshape.154
  396.2 4.8 %multiply_reduce_fusion = f32[128,2048]{1,0:T(8,128)S(1)} fusion(f32[128,2,2048]{2,1,0:T(2,128)} %reshape.154, f32[128,2]{1,0:T(8,128)S(1)} %copy.51), kind=kLoop, calls=%fused_computation.29 | loop fusion | flops 786432 | bytes 3146752 | tf_op jit(solution)/shard_map/reduce_sum | solution.py:136
  401.2 1.0 fusion.30
  (68 shorter events, 4.5 us)
Async XLA Ops:
  6.5 330.1 %copy-start = (bf16[1,512,2048]{2,1,0:T(8,128)(2,1)S(1)}, bf16[1,512,2048]{2,1,0:T(8,128)(2,1)}, u32[]{:S(2)}) copy-start(bf16[1,512,2048]{2,1,0:T(8,128)(2,1)} %param.31) | copy-start | bytes 6291460
  6.5 6.7 %copy-start.5 = (s32[128,2]{0,1:T(2,128)S(1)}, s32[128,2]{0,1:T(2,128)}, u32[]{:S(2)}) copy-start(s32[128,2]{0,1:T(2,128)} %param.27) | copy-start | bytes 3076
  6.5 77.3 %all-gather.2.cloned.1.call-start = ((), (), s32[]{:S(2)}) async-start(), calls=%async_computation.3 | async-start | bytes 8912896 | tf_op jit(solution)/shard_map/all_gather | solution.py:83
  95.8 15.5 %copy-start.1 = (bf16[128,2048]{1,0:T(8,128)(2,1)S(1)}, bf16[128,2048]{1,0:T(8,128)(2,1)}, u32[]{:S(2)}) copy-start(bf16[128,2048]{1,0:T(8,128)(2,1)} %param.22) | copy-start | bytes 1572868
  95.8 15.5 %copy-start.2 = (f32[2048]{0:T(1024)S(1)}, f32[2048]{0:T(1024)}, u32[]{:S(2)}) copy-start(f32[2048]{0:T(1024)} %param.24) | copy-start | bytes 24580
  96.6 11.6 %all-to-all-start = ((bf16[8,128,128]{1,2,0:T(8,128)(2,1)}), bf16[8,128,128]{1,2,0:T(8,128)(2,1)S(1)}, u32[]{:S(2)}, u32[]{:S(2)}) async-start(bf16[8,128,128]{1,2,0:T(8,128)(2,1)} %copy.45), calls=%async_computation | async-start | bytes 524288 | tf_op jit(solution)/shard_map/all_to_all | solution.py:102
  101.8 10.0 %copy-start.3 = (f32[2048]{0:T(1024)S(1)}, f32[2048]{0:T(1024)}, u32[]{:S(2)}) copy-start(f32[2048]{0:T(1024)} %param.25) | copy-start | bytes 24580
  341.9 11.0 %copy-start.6 = (f32[128,2]{0,1:T(2,128)S(1)}, f32[128,2]{0,1:T(2,128)}, u32[]{:S(2)}) copy-start(f32[128,2]{0,1:T(2,128)} %param.28) | copy-start | bytes 3076
  347.1 35.7 %all-to-all-start.2 = ((bf16[128,3,2048]{2,1,0:T(4,128)(2,1)}), bf16[128,3,2048]{2,1,0:T(4,128)(2,1)}, u32[]{:S(2)}, u32[]{:S(2)}) async-start(bf16[128,3,2048]{2,1,0:T(4,128)(2,1)} %reshape.152), calls=%async_computation.2 | async-start | bytes 4194304 | tf_op jit(solution)/shard_map/all_to_all | solution.py:127
  392.8 8.4 %copy-start.4 = (f32[2048]{0:T(1024)S(1)}, f32[2048]{0:T(1024)}, u32[]{:S(2)}) copy-start(f32[2048]{0:T(1024)} %param.26) | copy-start | bytes 24580
Sparse Core Ops, SparseCore 0:
  9.9 73.9 all-gather.1
where the time goes:
time: 411 us; the launch traced here: 409 us
  blocking collectives  203 us (49%)
  waiting for transfers between devices  107 us (26%)
  local copies, waits for them, and re-layouts  45.1 us (11%)
  matrix products  17.9 us (4%)
  between operations  13.6 us (3%)
  other arithmetic  11.6 us (3%)
  starting transfers between devices  10.9 us (3%)
    all_to_all x1, blocking collectives, local(): lax.all_to_all(outgoing, ('sp', 'tp'), split_axis=0, concat_axis=0, tiled...  203 us
    all_gather x1, waiting for transfers between devices, local(): piece = lax.all_gather(paired, 'sp', axis=1, tiled=True)  70.6 us
    all_to_all x1, waiting for transfers between devices, local(): lax.all_to_all(expert_out.reshape(sources, slots, width_here), ('sp', 'tp...  29.7 us
  transfers between devices with their start and end apart: 3, of which 3 were waited for; matrix products, arithmetic and copies ran while one was open for 1% of the time, Pallas kernels for 0%

commit v1 on v0

v1 whole, which is shorter than its diff:
```python
import functools

import jax
import jax.numpy as jnp
from jax import lax
from jax.experimental import pallas as pl
from jax.experimental.pallas import tpu as pltpu
from jax.sharding import PartitionSpec as P

HEAD_DIM = 64
NORM_EPS = 1e-06
MASKED = -1e30
BF = jnp.bfloat16
F32 = jnp.float32
ALL = ("sp", "tp")
BLK = 1024
TILE = 128
QG = 512


def member(k, z):
    return 4 * z + (k if z % 2 == 0 else 3 - k)


def group_of(sp):
    z, x = divmod(sp, 4)
    return x if z % 2 == 0 else 3 - x


def exchange_pairs(m1, m2):
    pairs = []
    for sp in range(16):
        z = sp // 4
        for tp in range(8):
            y, s = divmod(tp, 2)
            to_z = 2 * s + (m1 ^ (z & 1))
            to_c = m2 ^ (z >> 1)
            pairs.append((sp * 8 + tp, member(group_of(sp), to_z) * 8 + 2 * y + to_c))
    return pairs


def ring_pairs(step):
    return [(sp, 4 * (sp // 4) + (sp % 4 + step) % 4) for sp in range(16)]


def out_groups():
    return [
        [member(k, z) * 8 + 2 * y + c for z in range(4) for y in range(4)]
        for k in range(4)
        for c in range(2)
    ]


CORE_PAIRS = [(i, i ^ 1) for i in range(8)]


def pack_kernel(meta, q_ref, k_ref, v_ref, *outs):
    z = meta[0]
    row = lax.broadcasted_iota(jnp.int32, (128, 128), 0)
    col = lax.broadcasted_iota(jnp.int32, (128, 128), 1)
    for m1 in range(2):
        f1 = m1 ^ (z & 1)
        low = jnp.where((col < 64) & (row == col + 64 * f1), 1.0, 0.0)
        high = jnp.where((col >= 64) & (row == col - 64 + 64 * f1), 1.0, 0.0)
        sel_lo, sel_hi = low.astype(BF), high.astype(BF)
        q_lo, q_hi = (low * 0.125).astype(BF), (high * 0.125).astype(BF)

        def dot(a, b):
            return jnp.dot(a, b, preferred_element_type=F32)

        for m2 in range(2):
            f2 = m2 ^ (z >> 1)
            out = outs[2 * m1 + m2]
            for i in range(4):
                src = pl.ds(pl.multiple_of((2 * i + f2) * TILE, TILE), TILE)
                kv = dot(k_ref[src, :], sel_lo) + dot(v_ref[src, :], sel_hi)
                out[i * TILE : (i + 1) * TILE, :] = kv.astype(BF)
            for i in range(2):
                src_a = pl.ds(pl.multiple_of((2 * i + f2) * TILE, TILE), TILE)
                src_b = pl.ds(pl.multiple_of((2 * i + 4 + f2) * TILE, TILE), TILE)
                qq = dot(q_ref[src_a, :], q_lo) + dot(q_ref[src_b, :], q_hi)
                out[QG + i * TILE : QG + (i + 1) * TILE, :] = qq.astype(BF)


def pack(meta, q, k, v):
    return pl.pallas_call(
        pack_kernel,
        in_specs=[pl.BlockSpec(memory_space=pltpu.SMEM)] + [pl.BlockSpec(memory_space=pltpu.VMEM)] * 3,
        out_shape=[jax.ShapeDtypeStruct((768, 128), BF)] * 4,
        out_specs=[pl.BlockSpec(memory_space=pltpu.VMEM)] * 4,
        name="pack",
    )(meta, q, k, v)


def attend_kernel(n_pairs, first, last, meta, *refs):
    refs = list(refs)
    gate_own, gate_peer = refs.pop(0), refs.pop(0)
    qs = [refs.pop(0) for _ in range(4)]
    kv_in = [refs.pop(0) for _ in range(2 * n_pairs)]
    if not first:
        m_in, acc_in = refs.pop(0), refs.pop(0)
    if last:
        out_ref = refs.pop(0)
        m_ref, acc_ref = None, None
    else:
        m_ref, acc_ref = refs.pop(0), refs.pop(0)
    kv, q_pad, gate, sems = refs.pop(0), refs.pop(0), refs.pop(0), refs.pop(0)
    if last:
        m_ref, acc_ref = refs.pop(0), refs.pop(0)
    z, x, core = meta[0], meta[1], meta[2]

    copies = []
    for i, src in enumerate(kv_in):
        copies.append(pltpu.make_async_copy(src, kv.at[pl.ds(i * 2048, 2048)], sems.at[i]))
        copies[-1].start()

    mine = lax.shift_right_logical(z, 1) == core
    row0 = pl.multiple_of((z & 1) * 128, 128)
    gate[...] = jnp.where(mine, gate_own[pl.ds(row0, 128), :], gate_peer[pl.ds(row0, 128), :])

    lane = lax.broadcasted_iota(jnp.int32, (256, 128), 1)
    for g in range(4):
        packed = qs[g][...].astype(F32)
        q_pad[g, 0:256, :] = jnp.where(lane < 64, packed, 0.0).astype(BF)
        q_pad[g, 256:512, :] = jnp.where(lane < 64, pltpu.roll(packed, 64, 1), 0.0).astype(BF)
    if first:
        m_ref[...] = jnp.full(m_ref.shape, MASKED, F32)
        acc_ref[...] = jnp.zeros(acc_ref.shape, F32)
    else:
        m_ref[...] = m_in[...]
        acc_ref[...] = acc_in[...]

    def block_of(m1, m2, parity, x_of):
        zb = (m1 ^ (z & 1)) + 2 * (m2 ^ parity)
        xb = jnp.where(m1 == 1, 3 - x_of, x_of)
        return zb, 4 * zb + xb

    def step(g, base, m1, m2, b_q, b_k, masked):
        start_a = pl.multiple_of(base + (2 * m1 + m2) * QG, QG)
        start_b = pl.multiple_of(base + 2048 + (2 * m1 + (1 - m2)) * QG, QG)
        kv_a, kv_b = kv[pl.ds(start_a, QG), :], kv[pl.ds(start_b, QG), :]
        ones = lax.broadcasted_iota(jnp.int32, (QG, 128), 1) < 64
        v_a = jnp.where(ones, jnp.ones_like(kv_a), kv_a)
        v_b = jnp.where(ones, jnp.ones_like(kv_b), kv_b)
        ref_gate = gate[pl.ds(b_q * 8, 1), 0:1]

        def gates(parity):
            parts = [gate[pl.ds(b_k * 8 + 2 * i + parity, 1), :] for i in range(4)]
            return jnp.concatenate(parts, axis=1) - ref_gate

        g_a, g_b = gates(core), gates(1 - core)
        for sub in range(2):
            rows = slice(sub * 256, sub * 256 + 256)
            q = q_pad[g, rows, :]
            nt = (((1,), (1,)), ((), ()))
            s_a = lax.dot_general(q, kv_a, nt, preferred_element_type=F32) - g_a
            s_b = lax.dot_general(q, kv_b, nt, preferred_element_type=F32) - g_b
            if masked:
                r = lax.broadcasted_iota(jnp.int32, (256, QG), 0) + sub * 256
                cc = lax.broadcasted_iota(jnp.int32, (256, QG), 1)
                qpos = lax.shift_right_logical(r, 7) * 256 + (r & 127) + core * 128
                kpos = lax.shift_right_logical(cc, 7) * 256 + (cc & 127)
                s_a = jnp.where(kpos + core * 128 <= qpos, s_a, MASKED)
                s_b = jnp.where(kpos + (1 - core) * 128 <= qpos, s_b, MASKED)
            m_old = m_ref[g, rows, :]
            top = jnp.maximum(jnp.max(s_a, axis=1, keepdims=True), jnp.max(s_b, axis=1, keepdims=True))
            m_new = jnp.maximum(m_old, top)
            m_col = m_new[:, 0:1]
            p_a = jnp.exp(s_a - m_col).astype(BF)
            p_b = jnp.exp(s_b - m_col).astype(BF)
            pv = jnp.dot(p_a, v_a, preferred_element_type=F32) + jnp.dot(p_b, v_b, preferred_element_type=F32)
            acc_ref[g, rows, :] = acc_ref[g, rows, :] * jnp.exp(m_old - m_new) + pv
            m_ref[g, rows, :] = m_new

    for i in range(n_pairs):
        copies[2 * i].wait()
        copies[2 * i + 1].wait()
        x_of = meta[3 + i]

        def body(t, _, i=i, x_of=x_of):
            g, slot = t // 4, t % 4
            _, b_q = block_of(g // 2, g % 2, core, x)
            _, b_k = block_of(slot // 2, slot % 2, core, x_of)

            @pl.when(b_k < b_q)
            def _():
                step(g, i * 4096, slot // 2, slot % 2, b_q, b_k, False)

            if first and i == 0:

                @pl.when(b_k == b_q)
                def _():
                    step(g, i * 4096, slot // 2, slot % 2, b_q, b_k, True)

            return 0

        lax.fori_loop(0, 16, body, 0)

    if last:

        def finish(g, _):
            zq, _b = block_of(g // 2, g % 2, core, x)
            lane64 = lax.broadcasted_iota(jnp.int32, (64, 128), 1) < 64
            for i in range(4):
                a = acc_ref[g, i * TILE : (i + 1) * TILE, :]
                o = a / a[:, 0:1]
                packed = jnp.where(lane64, pltpu.roll(o[0:64], 64, 1), o[64:128])
                out_ref[zq * 4 + i, :, :] = packed.astype(BF)
            return 0

        lax.fori_loop(0, 4, finish, 0)


def attend(meta, gates, qs, kvs, state=None, last=True):
    n_pairs = len(kvs) // 2
    first = state is None
    vmem = pl.BlockSpec(memory_space=pltpu.VMEM)
    hbm = pl.BlockSpec(memory_space=pl.ANY)
    args = [meta, *gates, *qs, *kvs]
    specs = [pl.BlockSpec(memory_space=pltpu.SMEM)] + [vmem] * 6 + [hbm] * len(kvs)
    if not first:
        args += list(state)
        specs += [vmem, vmem]
    pair = (4, QG, 128)
    if last:
        out_shape = jax.ShapeDtypeStruct((16, 64, 128), BF)
        out_specs = vmem
    else:
        out_shape = [jax.ShapeDtypeStruct(pair, F32)] * 2
        out_specs = [vmem, vmem]
    scratch = [
        pltpu.VMEM((4096 * n_pairs, 128), BF),
        pltpu.VMEM((4, QG, 128), BF),
        pltpu.VMEM((128, 128), F32),
        pltpu.SemaphoreType.DMA((2 * n_pairs,)),
    ]
    if last:
        scratch += [pltpu.VMEM(pair, F32), pltpu.VMEM(pair, F32)]
    return pl.pallas_call(
        functools.partial(attend_kernel, n_pairs, first, last),
        in_specs=specs,
        out_shape=out_shape,
        out_specs=out_specs,
        scratch_shapes=scratch,
        name="attend",
    )(*args)


def rms_scale(rows, gain):
    mean_sq = jnp.mean(rows * rows, axis=-1, keepdims=True)
    return rows * lax.rsqrt(mean_sq + NORM_EPS) * gain


def attention(queries, key_rows, value_rows, cum_gate):
    sp, tp = lax.axis_index("sp"), lax.axis_index("tp")
    z, x, core = sp // 4, sp % 4, tp % 2
    left, right, far = (x + 3) % 4, (x + 1) % 4, (x + 2) % 4
    gate_own = cum_gate.reshape(256, 128)
    gate_peer = lax.ppermute(gate_own, "tp", CORE_PAIRS)
    meta = jnp.stack([z, x, core, x, left, right, far]).astype(jnp.int32)
    msgs = pack(meta, queries, key_rows, value_rows)
    recv = [
        lax.ppermute(msgs[2 * m1 + m2], ALL, exchange_pairs(m1, m2))
        for m1 in range(2)
        for m2 in range(2)
    ]
    qs = [r[QG:] for r in recv]
    own = jnp.concatenate([r[:QG] for r in recv], axis=0)

    def swap(a):
        return lax.ppermute(a, "tp", CORE_PAIRS)

    from_left = lax.ppermute(own, "sp", ring_pairs(1))
    from_right = lax.ppermute(own, "sp", ring_pairs(-1))
    peer = swap(own)
    far_a = lax.ppermute(from_left[:1024], "sp", ring_pairs(1))
    far_b = lax.ppermute(from_right[1024:], "sp", ring_pairs(-1))
    left_peer, right_peer = swap(from_left), swap(from_right)
    far_own = jnp.concatenate([far_a, far_b], axis=0)
    far_peer = swap(far_own)
    out = attend(
        meta,
        (gate_own, gate_peer),
        qs,
        [own, peer, from_left, left_peer, from_right, right_peer, far_own, far_peer],
    )
    got = lax.all_to_all(out, ALL, split_axis=0, concat_axis=0, tiled=True, axis_index_groups=out_groups())
    got = got.reshape(4, 4, 64, 2, 64)
    return jnp.transpose(got, (3, 2, 1, 0, 4)).reshape(TILE, 1024)


def local(
    queries,
    key_rows,
    value_rows,
    cum_gate,
    residual,
    out_weight,
    gain_mix,
    gain_pre,
    gain_post,
    route_ids,
    route_weight,
    w_gate,
    w_up,
    w_down,
):
    head_rows = attention(queries, key_rows, value_rows, cum_gate)
    projected = jnp.dot(head_rows, out_weight, preferred_element_type=jnp.float32)
    stream = (residual.astype(jnp.float32) + rms_scale(projected, gain_mix)).astype(jnp.bfloat16)
    stream_wide = lax.optimization_barrier(stream).astype(jnp.float32)
    normed = rms_scale(stream_wide, gain_pre).astype(jnp.bfloat16)
    rows_dev, top_count = route_ids.shape
    model_width = normed.shape[1]
    experts_all = lax.axis_size("sp") * lax.axis_size("tp")
    capacity = max(2, (4 * rows_dev * top_count + 3 * experts_all - 1) // (3 * experts_all))
    flat_ids = route_ids.reshape(-1)
    onehot = (flat_ids[:, None] == lax.iota(jnp.int32, experts_all)[None, :]).astype(jnp.int32)
    slot_rank = jnp.sum(jnp.cumsum(onehot, axis=0) * onehot, axis=1) - 1
    slot_index = flat_ids * capacity + slot_rank
    spread = jnp.repeat(normed, top_count, axis=0)
    outgoing = (
        jnp.zeros((experts_all * capacity, model_width), jnp.bfloat16).at[slot_index].set(spread)
    )
    outgoing = outgoing.reshape(experts_all, capacity, model_width)
    arrived = lax.all_to_all(outgoing, ("sp", "tp"), split_axis=0, concat_axis=0, tiled=True)
    sources, slots, width_here = arrived.shape
    flat_rows = arrived.reshape(sources * slots, width_here)
    gate_act = jnp.dot(flat_rows, w_gate[0], preferred_element_type=jnp.float32)
    up_act = jnp.dot(flat_rows, w_up[0], preferred_element_type=jnp.float32)
    hidden = (jax.nn.silu(gate_act) * up_act).astype(jnp.bfloat16)
    expert_out = jnp.dot(hidden, w_down[0], preferred_element_type=jnp.float32).astype(jnp.bfloat16)
    returned = lax.all_to_all(
        expert_out.reshape(sources, slots, width_here),
        ("sp", "tp"),
        split_axis=0,
        concat_axis=0,
        tiled=True,
    )
    picked = returned.reshape(experts_all * capacity, model_width)[slot_index]
    picked = picked.reshape(rows_dev, top_count, model_width).astype(jnp.float32)
    combined = jnp.sum(picked * route_weight[:, :, None], axis=1)
    return (stream_wide + rms_scale(combined, gain_post)).astype(jnp.bfloat16)


def solution(mesh):
    return jax.shard_map(
        local,
        mesh=mesh,
        in_specs=(
            P("sp", "tp"),
            P("sp", "tp"),
            P("sp", "tp"),
            P("tp", None),
            P(("sp", "tp"), None),
            P(),
            P(),
            P(),
            P(),
            P(("sp", "tp"), None),
            P(("sp", "tp"), None),
            P(("sp", "tp"), None, None),
            P(("sp", "tp"), None, None),
            P(("sp", "tp"), None, None),
        ),
        out_specs=P(("sp", "tp"), None),
        check_vma=False,
    )
```

time: 411 us -> 256 us (0.62)
  blocking collectives: 203 us -> 36 us
  Pallas kernels: 0 us -> 51.8 us
  waiting for transfers between devices: 107 us -> 60.3 us
  starting transfers between devices: 10.9 us -> 32.9 us
  between operations: 13.6 us -> 0.42 us
  local copies, waits for them, and re-layouts: 45.1 us -> 52.9 us
  matrix products: 17.9 us -> 12.3 us
    all_to_all x1, blocking collectives: 203 us -> 36 us  [local(): lax.all_to_all(outgoing, ('sp', 'tp'), split_axis=0, concat_axis=0, tiled...]
    all_gather x1 -> x0, waiting for transfers between devices: 70.6 us -> none  [local(): piece = lax.all_gather(paired, 'sp', axis=1, tiled=True)]
    pallas_call x0 -> x2, Pallas kernels: none -> 51.8 us  [the longest x1 49.4 us: attend(): pl.pallas_call(functools.partial(attend_kernel, n_pairs, first, last), in...]
    ppermute x0 -> x13, waiting for transfers between devices: none -> 20.5 us  [the longest x1 9.25 us: attention(): from_left = lax.ppermute(own, 'sp', ring_pairs(1))]
    ppermute x0 -> x13, starting transfers between devices: none -> 17.1 us  [the longest x4 10.6 us: attention(): lax.ppermute(msgs[2 * m1 + m2], ALL, exchange_pairs(m1, m2))]
    slice x1 -> x10, local copies, waits for them, and re-layouts: 1.06 us -> 8.41 us  [the longest x4 5.88 us: attention(): qs = [r[QG:] for r in recv]]
    dot_general x2 -> x0, matrix products: 5.63 us -> none  [the longest x1 3.21 us: attend(): jnp.einsum('hqk,khd->qhd', unnorm.astype(jnp.bfloat16), value_part, prefe...]
    all_to_all x1, starting transfers between devices: 5.12 us -> 9.83 us  [attention(): lax.all_to_all(out, ALL, split_axis=0, concat_axis=0, tiled=True, axis_in...]
  transfers between devices with their start and end apart: 3 -> 15, of which waited for: 3 -> 8; matrix products, arithmetic and copies ran while one was open for 1% -> 6% of each run, Pallas kernels for 0% -> 0%
where the time goes in v1:
time: 256 us; the launch traced here: 254 us
  waiting for transfers between devices  60.3 us (24%)
  local copies, waits for them, and re-layouts  52.9 us (21%)
  Pallas kernels  51.8 us (20%)
  blocking collectives  36 us (14%)
  starting transfers between devices  32.9 us (13%)
  matrix products  12.3 us (5%)
  other arithmetic  7.79 us (3%)
    pallas_call x1, Pallas kernels, attend(): pl.pallas_call(functools.partial(attend_kernel, n_pairs, first, last), in...  49.4 us
    all_to_all x1, blocking collectives, local(): lax.all_to_all(outgoing, ('sp', 'tp'), split_axis=0, concat_axis=0, tiled...  36 us
    all_to_all x1, waiting for transfers between devices, local(): lax.all_to_all(expert_out.reshape(sources, slots, width_here), ('sp', 'tp...  29.7 us
    ppermute x4, starting transfers between devices, attention(): lax.ppermute(msgs[2 * m1 + m2], ALL, exchange_pairs(m1, m2))  10.6 us
    all_to_all x1, waiting for transfers between devices, attention(): lax.all_to_all(out, ALL, split_axis=0, concat_axis=0, tiled=True, axis_in...  10 us
    all_to_all x1, starting transfers between devices, attention(): lax.all_to_all(out, ALL, split_axis=0, concat_axis=0, tiled=True, axis_in...  9.83 us
    ppermute x1, waiting for transfers between devices, attention(): from_left = lax.ppermute(own, 'sp', ring_pairs(1))  9.25 us
    ppermute x4, waiting for transfers between devices, attention(): lax.ppermute(msgs[2 * m1 + m2], ALL, exchange_pairs(m1, m2))  7.96 us
  transfers between devices with their start and end apart: 15, of which 8 were waited for; matrix products, arithmetic and copies ran while one was open for 6% of the time, Pallas kernels for 0%

profile of v1, /device:TPU:1, one launch (start us, length us, event | category | flops | bytes accessed | tf_op | source)
XLA Modules:
  0.0 254.4 jit_solution(14165478796463529090)
XLA Ops:
  0.7 2.4 pack.1
  3.1 6.8 %collective-permute-start.4 = (bf16[768,128]{1,0:T(8,128)(2,1)}, bf16[768,128]{1,0:T(8,128)(2,1)S(1)}, u32[]{:S(2)}, u32[]{:S(2)}) collective-permute-start(bf16[768,128]{1,0:T(8,128)(2,1)} %get-tuple-element.12), channel_id=1, source_target_pairs={{0,57},{1,121},{2,59},{3,123},{4,61},{5,125},{6,63},{7,127},{8,49}... | collective-permute-start | bytes 589832 | tf_op jit(solution)/shard_map/ppermute | solution.py:263
  11.7 2.1 collective-permute-start.1
  14.9 5.1 %collective-permute-done.3 = bf16[768,128]{1,0:T(8,128)(2,1)S(1)} collective-permute-done((bf16[768,128]{1,0:T(8,128)(2,1)}, bf16[768,128]{1,0:T(8,128)(2,1)S(1)}, u32[]{:S(2)}, u32[]{:S(2)}) %collective-permute-start.3) | collective-permute-done | bytes 196640 | tf_op jit(solution)/shard_map/ppermute | solution.py:263
  20.1 1.7 collective-permute-done.1
  22.6 2.7 %collective-permute-start.8 = (bf16[2048,128]{1,0:T(8,128)(2,1)S(1)}, bf16[2048,128]{1,0:T(8,128)(2,1)}, u32[]{:S(2)}, u32[]{:S(2)}) collective-permute-start(bf16[2048,128]{1,0:T(8,128)(2,1)S(1)} %pad_maximum_fusion.refs_6_), channel_id=1, source_target_pairs={{0,24},{8,0},{16,8},{24,16},{32,56},{40,32},{48,40},{56,48},{64,88... | collective-permute-start | bytes 1572872 | tf_op jit(solution)/shard_map/ppermute | solution.py:274
  25.9 9.3 %collective-permute-done.6.refs_8_ = bf16[2048,128]{1,0:T(8,128)(2,1)S(1)} collective-permute-done((bf16[2048,128]{1,0:T(8,128)(2,1)S(1)}, bf16[2048,128]{1,0:T(8,128)(2,1)S(1)}, u32[]{:S(2)}, u32[]{:S(2)}) %collective-permute-start.6) | collective-permute-done | bytes 524320 | tf_op jit(solution)/shard_map/ppermute | solution.py:273
  36.2 1.7 slice.59
  37.9 2.7 %collective-permute-start.11 = (bf16[1024,128]{1,0:T(8,128)(2,1)}, bf16[1024,128]{1,0:T(8,128)(2,1)}, u32[]{:S(2)}, u32[]{:S(2)}) collective-permute-start(bf16[1024,128]{1,0:T(8,128)(2,1)} %slice.59), channel_id=1, source_target_pairs={{0,24},{8,0},{16,8},{24,16},{32,56},{40,32},{48,40},{56,48},{64,88... | collective-permute-start | bytes 786440 | tf_op jit(solution)/shard_map/ppermute | solution.py:277
  41.2 3.2 %collective-permute-done.10 = bf16[1024,128]{1,0:T(8,128)(2,1)} collective-permute-done((bf16[1024,128]{1,0:T(8,128)(2,1)}, bf16[1024,128]{1,0:T(8,128)(2,1)}, u32[]{:S(2)}, u32[]{:S(2)}) %collective-permute-start.10) | collective-permute-done | bytes 262176 | tf_op jit(solution)/shard_map/ppermute | solution.py:276
  44.3 1.7 constant_dynamic-update-slice_fusion.1
  46.1 1.7 constant_dynamic-update-slice_fusion.refs_12_
  50.1 1.5 slice.50.refs_2_
  56.0 49.4 %attend.1 = bf16[16,64,128]{2,1,0:T(8,128)(2,1)} custom-call(s32[7]{0:T(128)} %stack.28.meta, f32[256,128]{1,0:T(8,128)} %copy-done.4, f32[256,128]{1,0:T(8,128)} %collective-permute-done.refs_1_, bf16[256,128]{1,0:T(8,128)(2,1)} %slice.50.refs_2_, bf16[256,128]{1,0:T(8,128)(2,1)} %slice.51.refs_3_, bf16[256,128]{1,0:T(8,128)(2,1)} %slice.52.refs_4_, ...), custom_call_target="tpu_custom_call" | custom-call | tf_op jit(solution)/shard_map/attend/pallas_call | solution.py:239
  105.5 9.8 %all-to-all-start = ((bf16[16,64,128]{2,1,0:T(8,128)(2,1)}), bf16[16,64,128]{2,1,0:T(8,128)(2,1)S(1)}, u32[]{:S(2)}, u32[]{:S(2)}) async-start(bf16[16,64,128]{2,1,0:T(8,128)(2,1)} %attend.1), calls=%async_computation | async-start | bytes 524288 | tf_op jit(solution)/shard_map/all_to_all | solution.py:287
  115.6 10.0 %all-to-all-done = bf16[16,64,128]{2,1,0:T(8,128)(2,1)S(1)} async-done(((bf16[16,64,128]{2,1,0:T(8,128)(2,1)}), bf16[16,64,128]{2,1,0:T(8,128)(2,1)S(1)}, u32[]{:S(2)}, u32[]{:S(2)}) %all-to-all-start) | async-done | bytes 262176 | tf_op jit(solution)/shard_map/all_to_all | solution.py:287
  126.7 3.0 %multiply_reduce_fusion.2 = (f32[128]{0:T(128)S(1)}, f32[128,2048]{1,0:T(8,128)S(1)}) fusion(bf16[128,1024]{1,0:T(8,128)(2,1)S(1)} %reshape.108, bf16[1024,2048]{1,0:T(8,128)(2,1)} %param.19), kind=kOutput, calls=%fused_computation.20 | convolution fusion | flops 537395072 | bytes 5505536 | tf_op jit(solution)/shard_map/dot_general | solution.py:309
  130.6 1.6 broadcast_in_dim.5
  132.2 2.2 reshape.128
  134.5 4.1 %scatter_custom_fusion = bf16[384,2048]{1,0:T(8,128)(2,1)} fusion(s32[256]{0:T(256)S(1)} %bitcast.45, bf16[256,2048]{1,0:T(8,128)(2,1)} %reshape.128, bf16[]{:T(256)} %constant.79.clone.1), kind=kCustom, calls=%fused_computation.26 | custom fusion | bytes 1573376 | tf_op jit(solution)/shard_map/scatter | solution.py:323
  138.6 5.1 %reshape.111 = bf16[128,3,2048]{2,1,0:T(4,128)(2,1)} reshape(bf16[384,2048]{1,0:T(8,128)(2,1)} %scatter_custom_fusion) | data formatting | bytes 3145728 | tf_op jit(solution)/shard_map/reshape | solution.py:325
  143.7 36.0 %all_to_all.15 = bf16[128,3,2048]{2,1,0:T(4,128)(2,1)} all-to-all(bf16[128,3,2048]{2,1,0:T(4,128)(2,1)} %reshape.111), channel_id=1, replica_groups=mesh['sp'=16,'tp'=8] {'sp','tp'}, dimensions={0} | all-to-all | bytes 3145728 | tf_op jit(solution)/shard_map/all_to_all | solution.py:326
  179.8 5.0 %reshape.112 = bf16[384,2048]{1,0:T(8,128)(2,1)} reshape(bf16[128,3,2048]{2,1,0:T(4,128)(2,1)} %all_to_all.15) | data formatting | bytes 3145728 | tf_op jit(solution)/shard_map/reshape | solution.py:328
  184.8 3.9 %fusion.3 = f32[384,512]{1,0:T(8,128)} fusion(bf16[384,2048]{1,0:T(8,128)(2,1)} %reshape.112, bf16[1,2048,512]{2,1,0:T(8,128)(2,1)} %param.25), kind=kOutput, calls=%fused_computation.6 | convolution fusion | flops 805306368 | bytes 4456448 | tf_op jit(solution)/shard_map/dot_general | solution.py:329
  188.8 5.3 %convolution_convert_fusion = bf16[384,2048]{1,0:T(8,128)(2,1)} fusion(bf16[1,512,2048]{2,1,0:T(8,128)(2,1)S(1)} %copy-done, bf16[384,2048]{1,0:T(8,128)(2,1)} %reshape.112, bf16[1,2048,512]{2,1,0:T(8,128)(2,1)} %param.26, f32[384,512]{1,0:T(8,128)} %fusion.3), kind=kOutput, calls=%fused_computation.2 | convolution fusion | flops 1612578816 | bytes 8126464 | tf_op jit(solution)/shard_map/dot_general | solution.py:332
  194.1 5.1 %reshape.113 = bf16[128,3,2048]{2,1,0:T(4,128)(2,1)} reshape(bf16[384,2048]{1,0:T(8,128)(2,1)} %convolution_convert_fusion) | data formatting | bytes 3145728 | tf_op jit(solution)/shard_map/reshape | solution.py:334
  199.2 5.9 %all-to-all-start.2 = ((bf16[128,3,2048]{2,1,0:T(4,128)(2,1)}), bf16[128,3,2048]{2,1,0:T(4,128)(2,1)}, u32[]{:S(2)}, u32[]{:S(2)}) async-start(bf16[128,3,2048]{2,1,0:T(4,128)(2,1)} %reshape.113), calls=%async_computation.2 | async-start | bytes 4194304 | tf_op jit(solution)/shard_map/all_to_all | solution.py:333
  205.3 29.7 %all-to-all-done.2 = bf16[128,3,2048]{2,1,0:T(4,128)(2,1)} async-done(((bf16[128,3,2048]{2,1,0:T(4,128)(2,1)}), bf16[128,3,2048]{2,1,0:T(4,128)(2,1)}, u32[]{:S(2)}, u32[]{:S(2)}) %all-to-all-start.2) | async-done | bytes 1572896 | tf_op jit(solution)/shard_map/all_to_all | solution.py:333
  235.0 5.0 %reshape.114 = bf16[384,2048]{1,0:T(8,128)(2,1)} reshape(bf16[128,3,2048]{2,1,0:T(4,128)(2,1)} %all-to-all-done.2) | data formatting | bytes 3145728 | tf_op jit(solution)/shard_map/reshape | solution.py:340
  240.1 4.9 %gather_fusion = bf16[256,2048]{1,0:T(8,128)(2,1)} fusion(bf16[384,2048]{1,0:T(8,128)(2,1)} %reshape.114, s32[1024]{0:T(1024)S(1)} %pad_clamp_fusion), kind=kCustom, calls=%fused_computation | custom fusion | bytes 2098176 | tf_op jit(solution)/shard_map/gather | solution.py:340
  245.0 3.3 %reshape.115 = f32[128,2,2048]{2,1,0:T(2,128)} reshape(bf16[256,2048]{1,0:T(8,128)(2,1)} %gather_fusion) | data formatting | bytes 3145728 | tf_op jit(solution)/shard_map/convert_element_type | solution.py:341
  248.4 4.8 %multiply_reduce_fusion = f32[128,2048]{1,0:T(8,128)S(1)} fusion(f32[128,2,2048]{2,1,0:T(2,128)} %reshape.115, f32[128,2]{1,0:T(8,128)S(1)} %copy.22), kind=kLoop, calls=%fused_computation.8 | loop fusion | flops 786432 | bytes 3146752 | tf_op jit(solution)/shard_map/reduce_sum | solution.py:342
  (89 shorter events, 16.9 us)
Async XLA Ops:
  0.0 188.8 %copy-start = (bf16[1,512,2048]{2,1,0:T(8,128)(2,1)S(1)}, bf16[1,512,2048]{2,1,0:T(8,128)(2,1)}, u32[]{:S(2)}) copy-start(bf16[1,512,2048]{2,1,0:T(8,128)(2,1)} %param.27) | copy-start | bytes 6291460
  0.0 25.3 %copy-start.9 = (f32[2,16384]{1,0:T(2,128)S(1)}, f32[2,16384]{1,0:T(2,128)}, u32[]{:S(2)}) copy-start(f32[2,16384]{1,0:T(2,128)} %param.17) | copy-start | bytes 393220
  0.0 25.5 %copy-start.13 = (s32[128,2]{0,1:T(2,128)S(1)}, s32[128,2]{0,1:T(2,128)}, u32[]{:S(2)}) copy-start(s32[128,2]{0,1:T(2,128)} %param.23) | copy-start | bytes 3076
  3.1 11.8 %collective-permute-start.4 = (bf16[768,128]{1,0:T(8,128)(2,1)}, bf16[768,128]{1,0:T(8,128)(2,1)S(1)}, u32[]{:S(2)}, u32[]{:S(2)}) collective-permute-start(bf16[768,128]{1,0:T(8,128)(2,1)} %get-tuple-element.12), channel_id=1, source_target_pairs={{0,57},{1,121},{2,59},{3,123},{4,61},{5,125},{6,63},{7,127},{8,49}... | collective-permute-start | bytes 589832 | tf_op jit(solution)/shard_map/ppermute | solution.py:263
  9.9 10.2 %collective-permute-start.3 = (bf16[768,128]{1,0:T(8,128)(2,1)}, bf16[768,128]{1,0:T(8,128)(2,1)S(1)}, u32[]{:S(2)}, u32[]{:S(2)}) collective-permute-start(bf16[768,128]{1,0:T(8,128)(2,1)} %get-tuple-element.11), channel_id=1, source_target_pairs={{0,56},{1,120},{2,58},{3,122},{4,60},{5,124},{6,62},{7,126},{8,48}... | collective-permute-start | bytes 589832 | tf_op jit(solution)/shard_map/ppermute | solution.py:263
  10.4 9.6 %collective-permute-start.2 = (bf16[768,128]{1,0:T(8,128)(2,1)}, bf16[768,128]{1,0:T(8,128)(2,1)S(1)}, u32[]{:S(2)}, u32[]{:S(2)}) collective-permute-start(bf16[768,128]{1,0:T(8,128)(2,1)} %get-tuple-element.10), channel_id=1, source_target_pairs={{0,1},{1,65},{2,3},{3,67},{4,5},{5,69},{6,7},{7,71},{8,9},{9,73},{... | collective-permute-start | bytes 589832 | tf_op jit(solution)/shard_map/ppermute | solution.py:263
  11.7 10.1 %collective-permute-start.1 = (bf16[768,128]{1,0:T(8,128)(2,1)}, bf16[768,128]{1,0:T(8,128)(2,1)S(1)}, u32[]{:S(2)}, u32[]{:S(2)}) collective-permute-start(bf16[768,128]{1,0:T(8,128)(2,1)} %get-tuple-element.9), channel_id=1, source_target_pairs={{0,0},{1,64},{2,2},{3,66},{4,4},{5,68},{6,6},{7,70},{8,8},{9,72},{... | collective-permute-start | bytes 589832 | tf_op jit(solution)/shard_map/ppermute | solution.py:263
  14.9 6.9 %copy-start.5 = (bf16[768,128]{1,0:T(8,128)(2,1)}, bf16[768,128]{1,0:T(8,128)(2,1)S(1)}, u32[]{:S(2)}) copy-start(bf16[768,128]{1,0:T(8,128)(2,1)S(1)} %collective-permute-done.4) | copy-start | bytes 589828
  20.1 1.7 copy-start.6
  20.1 1.7 copy-start.7
  21.8 0.7 copy-start.8
  22.5 33.5 %copy-start.1 = (bf16[2048,128]{1,0:T(8,128)(2,1)}, bf16[2048,128]{1,0:T(8,128)(2,1)S(1)}, u32[]{:S(2)}) copy-start(bf16[2048,128]{1,0:T(8,128)(2,1)S(1)} %pad_maximum_fusion.refs_6_) | copy-start | bytes 1572868
  22.5 12.6 %collective-permute-start.6 = (bf16[2048,128]{1,0:T(8,128)(2,1)S(1)}, bf16[2048,128]{1,0:T(8,128)(2,1)S(1)}, u32[]{:S(2)}, u32[]{:S(2)}) collective-permute-start(bf16[2048,128]{1,0:T(8,128)(2,1)S(1)} %pad_maximum_fusion.refs_6_), channel_id=1, source_target_pairs={{0,8},{8,16},{16,24},{24,0},{32,40},{40,48},{48,56},{56,32},{64,72... | collective-permute-start | bytes 1572872 | tf_op jit(solution)/shard_map/ppermute | solution.py:273
  22.6 13.5 %collective-permute-start.8 = (bf16[2048,128]{1,0:T(8,128)(2,1)S(1)}, bf16[2048,128]{1,0:T(8,128)(2,1)}, u32[]{:S(2)}, u32[]{:S(2)}) collective-permute-start(bf16[2048,128]{1,0:T(8,128)(2,1)S(1)} %pad_maximum_fusion.refs_6_), channel_id=1, source_target_pairs={{0,24},{8,0},{16,8},{24,16},{32,56},{40,32},{48,40},{56,48},{64,88... | collective-permute-start | bytes 1572872 | tf_op jit(solution)/shard_map/ppermute | solution.py:274
  25.4 30.6 %copy-start.4 = (f32[256,128]{1,0:T(8,128)}, f32[256,128]{1,0:T(8,128)S(1)}, u32[]{:S(2)}) copy-start(f32[256,128]{1,0:T(8,128)S(1)} %reshape.106.refs_0_) | copy-start | bytes 393220
  25.4 30.6 %collective-permute-start = (f32[256,128]{1,0:T(8,128)S(1)}, f32[256,128]{1,0:T(8,128)}, u32[]{:S(2)}, u32[]{:S(2)}) collective-permute-start(f32[256,128]{1,0:T(8,128)S(1)} %reshape.106.refs_0_), channel_id=1, source_target_pairs={{0,1},{1,0},{2,3},{3,2},{4,5},{5,4},{6,7},{7,6},{8,9},{9,8},{10,11... | collective-permute-start | bytes 393224 | tf_op jit(solution)/shard_map/ppermute | solution.py:259
  35.1 20.9 %copy-start.2 = (bf16[2048,128]{1,0:T(8,128)(2,1)}, bf16[2048,128]{1,0:T(8,128)(2,1)S(1)}, u32[]{:S(2)}) copy-start(bf16[2048,128]{1,0:T(8,128)(2,1)S(1)} %collective-permute-done.6.refs_8_) | copy-start | bytes 1572868
  35.9 8.4 %collective-permute-start.10 = (bf16[1024,128]{1,0:T(8,128)(2,1)}, bf16[1024,128]{1,0:T(8,128)(2,1)}, u32[]{:S(2)}, u32[]{:S(2)}) collective-permute-start(bf16[1024,128]{1,0:T(8,128)(2,1)} %slice.58), channel_id=1, source_target_pairs={{0,8},{8,16},{16,24},{24,0},{32,40},{40,48},{48,56},{56,32},{64,72... | collective-permute-start | bytes 786440 | tf_op jit(solution)/shard_map/ppermute | solution.py:276
  37.9 8.2 %collective-permute-start.11 = (bf16[1024,128]{1,0:T(8,128)(2,1)}, bf16[1024,128]{1,0:T(8,128)(2,1)}, u32[]{:S(2)}, u32[]{:S(2)}) collective-permute-start(bf16[1024,128]{1,0:T(8,128)(2,1)} %slice.59), channel_id=1, source_target_pairs={{0,24},{8,0},{16,8},{24,16},{32,56},{40,32},{48,40},{56,48},{64,88... | collective-permute-start | bytes 786440 | tf_op jit(solution)/shard_map/ppermute | solution.py:277
  40.6 15.4 %collective-permute-start.5 = (bf16[2048,128]{1,0:T(8,128)(2,1)S(1)}, bf16[2048,128]{1,0:T(8,128)(2,1)}, u32[]{:S(2)}, u32[]{:S(2)}) collective-permute-start(bf16[2048,128]{1,0:T(8,128)(2,1)S(1)} %pad_maximum_fusion.refs_6_), channel_id=1, source_target_pairs={{0,1},{1,0},{2,3},{3,2},{4,5},{5,4},{6,7},{7,6},{8,9},{9,8},{10,11... | collective-permute-start | bytes 1572872 | tf_op jit(solution)/shard_map/ppermute | solution.py:271
  40.7 15.3 %collective-permute-start.7 = (bf16[2048,128]{1,0:T(8,128)(2,1)S(1)}, bf16[2048,128]{1,0:T(8,128)(2,1)}, u32[]{:S(2)}, u32[]{:S(2)}) collective-permute-start(bf16[2048,128]{1,0:T(8,128)(2,1)S(1)} %collective-permute-done.6.refs_8_), channel_id=1, source_target_pairs={{0,1},{1,0},{2,3},{3,2},{4,5},{5,4},{6,7},{7,6},{8,9},{9,8},{10,11... | collective-permute-start | bytes 1572872 | tf_op jit(solution)/shard_map/ppermute | solution.py:271
  44.3 11.7 %collective-permute-start.9 = (bf16[2048,128]{1,0:T(8,128)(2,1)}, bf16[2048,128]{1,0:T(8,128)(2,1)}, u32[]{:S(2)}, u32[]{:S(2)}) collective-permute-start(bf16[2048,128]{1,0:T(8,128)(2,1)} %collective-permute-done.8.refs_10_), channel_id=1, source_target_pairs={{0,1},{1,0},{2,3},{3,2},{4,5},{5,4},{6,7},{7,6},{8,9},{9,8},{10,11... | collective-permute-start | bytes 1572872 | tf_op jit(solution)/shard_map/ppermute | solution.py:271
  47.7 8.3 %collective-permute-start.12 = (bf16[2048,128]{1,0:T(8,128)(2,1)}, bf16[2048,128]{1,0:T(8,128)(2,1)}, u32[]{:S(2)}, u32[]{:S(2)}) collective-permute-start(bf16[2048,128]{1,0:T(8,128)(2,1)} %constant_dynamic-update-slice_fusion.refs_12_), channel_id=1, source_target_pairs={{0,1},{1,0},{2,3},{3,2},{4,5},{5,4},{6,7},{7,6},{8,9},{9,8},{10,11... | collective-permute-start | bytes 1572872 | tf_op jit(solution)/shard_map/ppermute | solution.py:271
  105.5 20.2 %all-to-all-start = ((bf16[16,64,128]{2,1,0:T(8,128)(2,1)}), bf16[16,64,128]{2,1,0:T(8,128)(2,1)S(1)}, u32[]{:S(2)}, u32[]{:S(2)}) async-start(bf16[16,64,128]{2,1,0:T(8,128)(2,1)} %attend.1), calls=%async_computation | async-start | bytes 524288 | tf_op jit(solution)/shard_map/all_to_all | solution.py:287
  126.6 3.1 %copy-start.3 = (bf16[128,2048]{1,0:T(8,128)(2,1)S(1)}, bf16[128,2048]{1,0:T(8,128)(2,1)}, u32[]{:S(2)}) copy-start(bf16[128,2048]{1,0:T(8,128)(2,1)} %param.18) | copy-start | bytes 1572868
  126.7 3.1 %copy-start.10 = (f32[2048]{0:T(1024)S(1)}, f32[2048]{0:T(1024)}, u32[]{:S(2)}) copy-start(f32[2048]{0:T(1024)} %param.20) | copy-start | bytes 24580
  129.7 0.7 copy-start.11
  199.2 6.0 %copy-start.14 = (f32[128,2]{0,1:T(2,128)S(1)}, f32[128,2]{0,1:T(2,128)}, u32[]{:S(2)}) copy-start(f32[128,2]{0,1:T(2,128)} %param.24) | copy-start | bytes 3076
  199.2 35.8 %all-to-all-start.2 = ((bf16[128,3,2048]{2,1,0:T(4,128)(2,1)}), bf16[128,3,2048]{2,1,0:T(4,128)(2,1)}, u32[]{:S(2)}, u32[]{:S(2)}) async-start(bf16[128,3,2048]{2,1,0:T(4,128)(2,1)} %reshape.113), calls=%async_computation.2 | async-start | bytes 4194304 | tf_op jit(solution)/shard_map/all_to_all | solution.py:333
  248.4 5.0 %copy-start.12 = (f32[2048]{0:T(1024)S(1)}, f32[2048]{0:T(1024)}, u32[]{:S(2)}) copy-start(f32[2048]{0:T(1024)} %param.22) | copy-start | bytes 24580

commit v2 on v1

--- a/solution.py
+++ b/solution.py
@@ -251,6 +251,163 @@
     return rows * lax.rsqrt(mean_sq + NORM_EPS) * gain
 
 
+PITCH = 24
+
+
+def slots_of(ids):
+    expert = lax.broadcasted_iota(jnp.int32, (TILE, 128), 1)
+    first = (ids[:, 0:1] == expert).astype(F32)
+    second = (ids[:, 1:2] == expert).astype(F32)
+    named = first + second
+    r = lax.broadcasted_iota(jnp.int32, (TILE, TILE), 0)
+    c = lax.broadcasted_iota(jnp.int32, (TILE, TILE), 1)
+    before = jnp.where(c < r, 1.0, 0.0).astype(BF)
+    rank = jnp.dot(before, named.astype(BF), preferred_element_type=F32)
+    return first, second, named, rank
+
+
+def mix_kernel(got, w_out, residual, gain_mix, gain_pre, ids, stream, outgoing, x, proj, normed, scr):
+    lane = lax.broadcasted_iota(jnp.int32, (64, 128), 1) < 64
+    for hp in range(8):
+        even, odd = 2 * hp, 2 * hp + 1
+
+        def block(h):
+            return got[(h % 4) * 4 + h // 4].astype(F32)
+
+        e, o = block(even), block(odd)
+        cols = slice(hp * 128, hp * 128 + 128)
+        x[0:64, cols] = jnp.where(lane, e, pltpu.roll(o, 64, 1)).astype(BF)
+        x[64:128, cols] = jnp.where(lane, pltpu.roll(e, 64, 1), o).astype(BF)
+    proj[...] = jnp.dot(x[...], w_out[...], preferred_element_type=F32)
+
+    def norm(i, _):
+        rows = pl.ds(pl.multiple_of(i * 16, 16), 16)
+        mixed = residual[rows, :].astype(F32) + rms_scale(proj[rows, :], gain_mix[...])
+        rounded = mixed.astype(BF)
+        stream[rows, :] = rounded
+        normed[rows, :] = rms_scale(rounded.astype(F32), gain_pre[...]).astype(BF)
+        return 0
+
+    lax.fori_loop(0, 8, norm, 0)
+
+    _, _, named, rank = slots_of(ids[...])
+    tn = (((0,), (0,)), ((), ()))
+    for s in range(3):
+        sel = jnp.where(rank == s, named, 0.0).astype(BF)
+        for j in range(0, 16, 2):
+            part = normed[:, j * 128 : j * 128 + 256]
+            res = lax.dot_general(sel, part, tn, preferred_element_type=F32)
+            scr[pl.ds(s * 128 * PITCH + j, 128, stride=PITCH), :] = res[:, 0:128]
+            scr[pl.ds(s * 128 * PITCH + j + 1, 128, stride=PITCH), :] = res[:, 128:256]
+
+    def put(e, _):
+        for s in range(3):
+            src = pl.multiple_of((s * 128 + e) * PITCH, 8)
+            dst = pl.multiple_of(e * 48 + s * 16, 16)
+            outgoing[pl.ds(dst, 16), :] = scr[pl.ds(src, 16), :].astype(BF)
+        return 0
+
+    lax.fori_loop(0, 128, put, 0, unroll=4)
+
+
+def mix(got, w_out, residual, gain_mix, gain_pre, ids):
+    vmem = pl.BlockSpec(memory_space=pltpu.VMEM)
+    return pl.pallas_call(
+        mix_kernel,
+        in_specs=[vmem] * 6,
+        out_shape=[jax.ShapeDtypeStruct((TILE, 2048), BF), jax.ShapeDtypeStruct((6144, 128), BF)],
+        out_specs=[vmem, vmem],
+        scratch_shapes=[
+            pltpu.VMEM((TILE, 1024), BF),
+            pltpu.VMEM((TILE, 2048), F32),
+            pltpu.VMEM((TILE, 2048), BF),
+            pltpu.VMEM((384 * PITCH, 128), F32),
+        ],
+        name="mix",
+    )(got, w_out, residual, gain_mix.reshape(1, -1), gain_pre.reshape(1, -1), ids)
+
+
+def expert_kernel(arrived, w_gate, w_up, w_down, out, scr, x):
+    def take(r, _):
+        src = pl.multiple_of(r * 16, 16)
+        scr[pl.ds(pl.multiple_of(r * PITCH, 8), 16), :] = arrived[pl.ds(src, 16), :].astype(F32)
+        return 0
+
+    lax.fori_loop(0, 384, take, 0, unroll=8)
+    for j in range(16):
+        x[:, j * 128 : j * 128 + 128] = scr[pl.ds(j, 384, stride=PITCH), :].astype(BF)
+    gate_act = jnp.dot(x[...], w_gate[0], preferred_element_type=F32)
+    up_act = jnp.dot(x[...], w_up[0], preferred_element_type=F32)
+    hidden = (jax.nn.silu(gate_act) * up_act).astype(BF)
+    for j in range(0, 16, 2):
+        res = jnp.dot(hidden, w_down[0, :, j * 128 : j * 128 + 256], preferred_element_type=F32)
+        scr[pl.ds(j, 384, stride=PITCH), :] = res[:, 0:128]
+        scr[pl.ds(j + 1, 384, stride=PITCH), :] = res[:, 128:256]
+
+    def put(r, _):
+        dst = pl.multiple_of(r * 16, 16)
+        out[pl.ds(dst, 16), :] = scr[pl.ds(pl.multiple_of(r * PITCH, 8), 16), :].astype(BF)
+        return 0
+
+    lax.fori_loop(0, 384, put, 0, unroll=8)
+
+
+def expert(arrived, w_gate, w_up, w_down):
+    vmem = pl.BlockSpec(memory_space=pltpu.VMEM)
+    return pl.pallas_call(
+        expert_kernel,
+        in_specs=[vmem] * 4,
+        out_shape=jax.ShapeDtypeStruct((6144, 128), BF),
+        out_specs=vmem,
+        scratch_shapes=[pltpu.VMEM((384 * PITCH, 128), F32), pltpu.VMEM((384, 2048), BF)],
+        name="expert",
+    )(arrived, w_gate, w_up, w_down)
+
+
+def combine_kernel(returned, stream, ids, weight, gain_post, out, scr, comb):
+    def take(e, _):
+        for s in range(3):
+            src = pl.multiple_of(e * 48 + s * 16, 16)
+            dst = pl.multiple_of((s * 128 + e) * PITCH, 8)
+            scr[pl.ds(dst, 16), :] = returned[pl.ds(src, 16), :].astype(F32)
+        return 0
+
+    lax.fori_loop(0, 128, take, 0, unroll=4)
+    first, second, _, rank = slots_of(ids[...])
+    w = weight[...]
+    share = first * w[:, 0:1] + second * w[:, 1:2]
+    full = jnp.concatenate([jnp.where(rank == s, share, 0.0) for s in range(3)], axis=1)
+    hi = full.astype(BF)
+    rest = full - hi.astype(F32)
+    mid = rest.astype(BF)
+    low = (rest - mid.astype(F32)).astype(BF)
+    for j in range(16):
+        rows = scr[pl.ds(j, 384, stride=PITCH), :].astype(BF)
+        res = jnp.dot(low, rows, preferred_element_type=F32)
+        res += jnp.dot(mid, rows, preferred_element_type=F32)
+        res += jnp.dot(hi, rows, preferred_element_type=F32)
+        comb[:, j * 128 : j * 128 + 128] = res
+
+    def norm(i, _):
+        rows = pl.ds(pl.multiple_of(i * 16, 16), 16)
+        out[rows, :] = (stream[rows, :].astype(F32) + rms_scale(comb[rows, :], gain_post[...])).astype(BF)
+        return 0
+
+    lax.fori_loop(0, 8, norm, 0)
+
+
+def combine(returned, stream, ids, weight, gain_post):
+    vmem = pl.BlockSpec(memory_space=pltpu.VMEM)
+    return pl.pallas_call(
+        combine_kernel,
+        in_specs=[vmem] * 5,
+        out_shape=jax.ShapeDtypeStruct((TILE, 2048), BF),
+        out_specs=vmem,
+        scratch_shapes=[pltpu.VMEM((384 * PITCH, 128), F32), pltpu.VMEM((TILE, 2048), F32)],
+        name="combine",
+    )(returned, stream, ids, weight, gain_post.reshape(1, -1))
+
+
 def attention(queries, key_rows, value_rows, cum_gate):
     sp, tp = lax.axis_index("sp"), lax.axis_index("tp")
     z, x, core = sp // 4, sp % 4, tp % 2
@@ -285,8 +442,7 @@
         [own, peer, from_left, left_peer, from_right, right_peer, far_own, far_peer],
     )
     got = lax.all_to_all(out, ALL, split_axis=0, concat_axis=0, tiled=True, axis_index_groups=out_groups())
-    got = got.reshape(4, 4, 64, 2, 64)
-    return jnp.transpose(got, (3, 2, 1, 0, 4)).reshape(TILE, 1024)
+    return got
 
 
 def local(
@@ -305,42 +461,16 @@
     w_up,
     w_down,
 ):
-    head_rows = attention(queries, key_rows, value_rows, cum_gate)
-    projected = jnp.dot(head_rows, out_weight, preferred_element_type=jnp.float32)
-    stream = (residual.astype(jnp.float32) + rms_scale(projected, gain_mix)).astype(jnp.bfloat16)
-    stream_wide = lax.optimization_barrier(stream).astype(jnp.float32)
-    normed = rms_scale(stream_wide, gain_pre).astype(jnp.bfloat16)
-    rows_dev, top_count = route_ids.shape
-    model_width = normed.shape[1]
-    experts_all = lax.axis_size("sp") * lax.axis_size("tp")
-    capacity = max(2, (4 * rows_dev * top_count + 3 * experts_all - 1) // (3 * experts_all))
-    flat_ids = route_ids.reshape(-1)
-    onehot = (flat_ids[:, None] == lax.iota(jnp.int32, experts_all)[None, :]).astype(jnp.int32)
-    slot_rank = jnp.sum(jnp.cumsum(onehot, axis=0) * onehot, axis=1) - 1
-    slot_index = flat_ids * capacity + slot_rank
-    spread = jnp.repeat(normed, top_count, axis=0)
-    outgoing = (
-        jnp.zeros((experts_all * capacity, model_width), jnp.bfloat16).at[slot_index].set(spread)
-    )
-    outgoing = outgoing.reshape(experts_all, capacity, model_width)
-    arrived = lax.all_to_all(outgoing, ("sp", "tp"), split_axis=0, concat_axis=0, tiled=True)
-    sources, slots, width_here = arrived.shape
-    flat_rows = arrived.reshape(sources * slots, width_here)
-    gate_act = jnp.dot(flat_rows, w_gate[0], preferred_element_type=jnp.float32)
-    up_act = jnp.dot(flat_rows, w_up[0], preferred_element_type=jnp.float32)
-    hidden = (jax.nn.silu(gate_act) * up_act).astype(jnp.bfloat16)
-    expert_out = jnp.dot(hidden, w_down[0], preferred_element_type=jnp.float32).astype(jnp.bfloat16)
-    returned = lax.all_to_all(
-        expert_out.reshape(sources, slots, width_here),
-        ("sp", "tp"),
-        split_axis=0,
-        concat_axis=0,
-        tiled=True,
-    )
-    picked = returned.reshape(experts_all * capacity, model_width)[slot_index]
-    picked = picked.reshape(rows_dev, top_count, model_width).astype(jnp.float32)
-    combined = jnp.sum(picked * route_weight[:, :, None], axis=1)
-    return (stream_wide + rms_scale(combined, gain_post)).astype(jnp.bfloat16)
+    got = attention(queries, key_rows, value_rows, cum_gate)
+
+    def exchange(rows):
+        moved = lax.all_to_all(rows.reshape(128, 48, 128), ALL, split_axis=0, concat_axis=0, tiled=True)
+        return moved.reshape(6144, 128)
+
+    stream, outgoing = mix(got, out_weight, residual, gain_mix, gain_pre, route_ids)
+    arrived = exchange(outgoing)
+    returned = exchange(expert(arrived, w_gate, w_up, w_down))
+    return combine(returned, stream, route_ids, route_weight, gain_post)
 
 
 def solution(mesh):

time: 256 us -> 205 us (0.80)
  local copies, waits for them, and re-layouts: 52.9 us -> 11.9 us
  Pallas kernels: 51.8 us -> 74.3 us
  matrix products: 12.3 us -> 0 us
  other arithmetic: 7.79 us -> 0.04 us
  blocking collectives: 36 us -> 30.7 us
  waiting for transfers between devices: 60.3 us -> 55.4 us
    reshape x8 -> x0, local copies, waits for them, and re-layouts: 23.6 us -> none  [the longest x1 5.14 us: local(): outgoing = outgoing.reshape(experts_all, capacity, model_width)]
    pallas_call x0 -> x3, Pallas kernels: none -> 22.5 us  [the longest x1 8.7 us: expert(): pl.pallas_call(expert_kernel, in_specs=[vmem] * 4, out_shape=jax.ShapeDty...]
    dot_general x3 -> x0, matrix products: 12.3 us -> none  [the longest x1 5.3 us: local(): jnp.dot(hidden, w_down[0], preferred_element_type=jnp.float32)]
    all_to_all x1, waiting for transfers between devices: 29.7 us -> 23.8 us  [exchange(): lax.all_to_all(rows.reshape(128, 48, 128), ALL, split_axis=0, concat_axis...]
    reduce_sum x4 -> x0, other arithmetic: 5.33 us -> none  [the longest x1 4.81 us: local(): combined = jnp.sum(picked * route_weight[:, :, None], axis=1)]
    all_to_all x1, blocking collectives: 36 us -> 30.7 us  [exchange(): lax.all_to_all(rows.reshape(128, 48, 128), ALL, split_axis=0, concat_axis...]
    gather x1 -> x0, local copies, waits for them, and re-layouts: 4.94 us -> none  [local(): picked = returned.reshape(experts_all * capacity, model_width)[slot_index]]
    scatter x1 -> x0, local copies, waits for them, and re-layouts: 4.13 us -> none  [local(): jnp.zeros((experts_all * capacity, model_width), jnp.bfloat16)]
  transfers between devices with their start and end apart: 15 -> 15, of which waited for: 8 -> 8; matrix products, arithmetic and copies ran while one was open for 6% -> 4% of each run, Pallas kernels for 0% -> 0%
where the time goes in v2:
time: 205 us
  Pallas kernels  74.3 us (36%)
  waiting for transfers between devices  55.4 us (27%)
  starting transfers between devices  32.1 us (16%)
  blocking collectives  30.7 us (15%)
  local copies, waits for them, and re-layouts  11.9 us (6%)
    pallas_call x1, Pallas kernels, attend(): pl.pallas_call(functools.partial(attend_kernel, n_pairs, first, last), in...  49.4 us
    all_to_all x1, blocking collectives, exchange(): lax.all_to_all(rows.reshape(128, 48, 128), ALL, split_axis=0, concat_axis...  30.7 us
    all_to_all x1, waiting for transfers between devices, exchange(): lax.all_to_all(rows.reshape(128, 48, 128), ALL, split_axis=0, concat_axis...  23.8 us
    ppermute x4, starting transfers between devices, attention(): lax.ppermute(msgs[2 * m1 + m2], ALL, exchange_pairs(m1, m2))  10.6 us
    ppermute x1, waiting for transfers between devices, attention(): from_left = lax.ppermute(own, 'sp', ring_pairs(1))  9.85 us
    all_to_all x1, starting transfers between devices, attention(): lax.all_to_all(out, ALL, split_axis=0, concat_axis=0, tiled=True, axis_in...  9.72 us
    all_to_all x1, waiting for transfers between devices, attention(): lax.all_to_all(out, ALL, split_axis=0, concat_axis=0, tiled=True, axis_in...  9.15 us
    pallas_call x1, Pallas kernels, expert(): pl.pallas_call(expert_kernel, in_specs=[vmem] * 4, out_shape=jax.ShapeDty...  8.7 us
  transfers between devices with their start and end apart: 15, of which 8 were waited for; matrix products, arithmetic and copies ran while one was open for 4% of the time, Pallas kernels for 0%

profile of v2, /device:TPU:1, one launch (start us, length us, event | category | flops | bytes accessed | tf_op | source)
XLA Modules:
  0.0 204.7 jit_solution(10011909327123419606)
XLA Ops:
  0.0 0.6 stack.28.meta
  0.6 2.4 %pack.1 = (bf16[768,128]{1,0:T(8,128)(2,1)}, bf16[768,128]{1,0:T(8,128)(2,1)}, bf16[768,128]{1,0:T(8,128)(2,1)}, bf16[768,128]{1,0:T(8,128)(2,1)}) custom-call(s32[7]{0:T(128)} %stack.28.meta, bf16[1024,128]{1,0:T(8,128)(2,1)} %q_ref.1, bf16[1024,128]{1,0:T(8,128)(2,1)} %k_ref.1, bf16[1024,128]{1,0:T(8,128)(2,1)} %v_ref.1), custom_call_target="tpu_custom_call" | custom-call | tf_op jit(solution)/shard_map/pack/pallas_call | solution.py:86
  3.0 6.8 %collective-permute-start.4 = (bf16[768,128]{1,0:T(8,128)(2,1)}, bf16[768,128]{1,0:T(8,128)(2,1)S(1)}, u32[]{:S(2)}, u32[]{:S(2)}) collective-permute-start(bf16[768,128]{1,0:T(8,128)(2,1)} %get-tuple-element.14), channel_id=1, source_target_pairs={{0,57},{1,121},{2,59},{3,123},{4,61},{5,125},{6,63},{7,127},{8,49}... | collective-permute-start | bytes 589832 | tf_op jit(solution)/shard_map/ppermute | solution.py:420
  10.3 1.2 collective-permute-start.2
  11.5 2.1 %collective-permute-start.1 = (bf16[768,128]{1,0:T(8,128)(2,1)}, bf16[768,128]{1,0:T(8,128)(2,1)S(1)}, u32[]{:S(2)}, u32[]{:S(2)}) collective-permute-start(bf16[768,128]{1,0:T(8,128)(2,1)} %get-tuple-element.11), channel_id=1, source_target_pairs={{0,0},{1,64},{2,2},{3,66},{4,4},{5,68},{6,6},{7,70},{8,8},{9,72},{... | collective-permute-start | bytes 589832 | tf_op jit(solution)/shard_map/ppermute | solution.py:420
  13.6 1.2 collective-permute-done.4
  14.8 5.1 %collective-permute-done.3 = bf16[768,128]{1,0:T(8,128)(2,1)S(1)} collective-permute-done((bf16[768,128]{1,0:T(8,128)(2,1)}, bf16[768,128]{1,0:T(8,128)(2,1)S(1)}, u32[]{:S(2)}, u32[]{:S(2)}) %collective-permute-start.3) | collective-permute-done | bytes 196640 | tf_op jit(solution)/shard_map/ppermute | solution.py:420
  20.0 1.7 collective-permute-done.1
  21.7 0.7 copy-done.11
  22.5 2.7 %collective-permute-start.8 = (bf16[2048,128]{1,0:T(8,128)(2,1)S(1)}, bf16[2048,128]{1,0:T(8,128)(2,1)S(1)}, u32[]{:S(2)}, u32[]{:S(2)}) collective-permute-start(bf16[2048,128]{1,0:T(8,128)(2,1)S(1)} %pad_maximum_fusion.refs_6_), channel_id=1, source_target_pairs={{0,24},{8,0},{16,8},{24,16},{32,56},{40,32},{48,40},{56,48},{64,88... | collective-permute-start | bytes 1572872 | tf_op jit(solution)/shard_map/ppermute | solution.py:431
  25.1 9.9 %collective-permute-done.6.refs_8_ = bf16[2048,128]{1,0:T(8,128)(2,1)S(1)} collective-permute-done((bf16[2048,128]{1,0:T(8,128)(2,1)S(1)}, bf16[2048,128]{1,0:T(8,128)(2,1)S(1)}, u32[]{:S(2)}, u32[]{:S(2)}) %collective-permute-start.6) | collective-permute-done | bytes 524320 | tf_op jit(solution)/shard_map/ppermute | solution.py:430
  35.1 2.9 %collective-permute-start.11 = (bf16[1024,128]{1,0:T(8,128)(2,1)S(1)}, bf16[1024,128]{1,0:T(8,128)(2,1)S(1)}, u32[]{:S(2)}, u32[]{:S(2)}) collective-permute-start(bf16[1024,128]{1,0:T(8,128)(2,1)S(1)} %slice.49), channel_id=1, source_target_pairs={{0,24},{8,0},{16,8},{24,16},{32,56},{40,32},{48,40},{56,48},{64,88... | collective-permute-start | bytes 786440 | tf_op jit(solution)/shard_map/ppermute | solution.py:434
  38.6 4.6 %collective-permute-done.10 = bf16[1024,128]{1,0:T(8,128)(2,1)S(1)} collective-permute-done((bf16[1024,128]{1,0:T(8,128)(2,1)S(1)}, bf16[1024,128]{1,0:T(8,128)(2,1)S(1)}, u32[]{:S(2)}, u32[]{:S(2)}) %collective-permute-start.10) | collective-permute-done | bytes 262176 | tf_op jit(solution)/shard_map/ppermute | solution.py:433
  43.4 1.1 reshape.24.refs_0_
  45.0 1.5 slice.40.refs_2_
  46.5 1.5 slice.41.refs_3_
  47.9 1.5 slice.42.refs_4_
  49.4 0.6 slice.43.refs_5_
  50.1 0.6 copy-done.12
  51.0 49.4 %attend.1 = bf16[16,64,128]{2,1,0:T(8,128)(2,1)} custom-call(s32[7]{0:T(128)} %stack.28.meta, f32[256,128]{1,0:T(8,128)} %copy-done.8, f32[256,128]{1,0:T(8,128)} %copy-done.12, bf16[256,128]{1,0:T(8,128)(2,1)} %slice.40.refs_2_, bf16[256,128]{1,0:T(8,128)(2,1)} %slice.41.refs_3_, bf16[256,128]{1,0:T(8,128)(2,1)} %slice.42.refs_4_, ...), custom_call_target="tpu_custom_call" | custom-call | tf_op jit(solution)/shard_map/attend/pallas_call | solution.py:239
  100.5 9.7 %all-to-all-start = ((bf16[16,64,128]{2,1,0:T(8,128)(2,1)}), bf16[16,64,128]{2,1,0:T(8,128)(2,1)S(1)}, u32[]{:S(2)}, u32[]{:S(2)}) async-start(bf16[16,64,128]{2,1,0:T(8,128)(2,1)} %attend.1), calls=%async_computation | async-start | bytes 524288 | tf_op jit(solution)/shard_map/all_to_all | solution.py:444
  110.2 0.7 copy.15.ids
  110.9 9.1 %all-to-all-done.got = bf16[16,64,128]{2,1,0:T(8,128)(2,1)S(1)} async-done(((bf16[16,64,128]{2,1,0:T(8,128)(2,1)}), bf16[16,64,128]{2,1,0:T(8,128)(2,1)S(1)}, u32[]{:S(2)}, u32[]{:S(2)}) %all-to-all-start) | async-done | bytes 262176 | tf_op jit(solution)/shard_map/all_to_all | solution.py:444
  120.1 0.7 copy-done.5
  120.8 8.0 %mix.1 = (bf16[128,2048]{1,0:T(8,128)(2,1)}, bf16[6144,128]{1,0:T(8,128)(2,1)}) custom-call(bf16[16,64,128]{2,1,0:T(8,128)(2,1)} %copy-done.5, bf16[1024,2048]{1,0:T(8,128)(2,1)} %w_out.1, bf16[128,2048]{1,0:T(8,128)(2,1)} %residual.1, f32[1,2048]{1,0:T(1,128)} %bitcast.17, f32[1,2048]{1,0:T(1,128)} %bitcast.18, s32[128,2]{1,0:T(8,128)} %copy.15.ids), custom_call_target="tpu_custom_call" | custom-call | tf_op jit(solution)/shard_map/mix/pallas_call | solution.py:315
  128.8 30.7 %all_to_all.15 = bf16[128,48,128]{2,1,0:T(8,128)(2,1)} all-to-all(bf16[128,48,128]{2,1,0:T(8,128)(2,1)} %bitcast.16), channel_id=1, replica_groups=mesh['sp'=16,'tp'=8] {'sp','tp'}, dimensions={0} | all-to-all | bytes 3145728 | tf_op jit(solution)/shard_map/all_to_all | solution.py:467
  159.5 8.7 %expert.1 = bf16[6144,128]{1,0:T(8,128)(2,1)} custom-call(bf16[6144,128]{1,0:T(8,128)(2,1)} %bitcast.14, bf16[1,2048,512]{2,1,0:T(8,128)(2,1)} %w_gate.1, bf16[1,2048,512]{2,1,0:T(8,128)(2,1)} %w_up.1, bf16[1,512,2048]{2,1,0:T(8,128)(2,1)} %w_down.1), custom_call_target="tpu_custom_call" | custom-call | tf_op jit(solution)/shard_map/expert/pallas_call | solution.py:357
  168.2 5.0 %all-to-all-start.2 = ((bf16[128,48,128]{2,1,0:T(8,128)(2,1)}), bf16[128,48,128]{2,1,0:T(8,128)(2,1)S(1)}, u32[]{:S(2)}, u32[]{:S(2)}) async-start(bf16[128,48,128]{2,1,0:T(8,128)(2,1)} %bitcast.13), calls=%async_computation.2 | async-start | bytes 3145728 | tf_op jit(solution)/shard_map/all_to_all | solution.py:467
  173.2 0.7 copy.17.weight
  174.0 23.8 %all-to-all-done.2 = bf16[128,48,128]{2,1,0:T(8,128)(2,1)S(1)} async-done(((bf16[128,48,128]{2,1,0:T(8,128)(2,1)}), bf16[128,48,128]{2,1,0:T(8,128)(2,1)S(1)}, u32[]{:S(2)}, u32[]{:S(2)}) %all-to-all-start.2) | async-done | bytes 1572896 | tf_op jit(solution)/shard_map/all_to_all | solution.py:467
  197.7 1.2 copy-done
  198.9 5.8 %combine.1 = bf16[128,2048]{1,0:T(8,128)(2,1)} custom-call(bf16[6144,128]{1,0:T(8,128)(2,1)} %bitcast.15, bf16[128,2048]{1,0:T(8,128)(2,1)} %get-tuple-element.16.stream, s32[128,2]{1,0:T(8,128)} %copy.15.ids, f32[128,2]{1,0:T(8,128)} %copy.17.weight, f32[1,2048]{1,0:T(1,128)} %bitcast.19), custom_call_target="tpu_custom_call" | custom-call | tf_op jit(solution)/shard_map/combine/pallas_call | solution.py:401
  (51 shorter events, 2.4 us)
Async XLA Ops:
  3.0 11.8 %collective-permute-start.4 = (bf16[768,128]{1,0:T(8,128)(2,1)}, bf16[768,128]{1,0:T(8,128)(2,1)S(1)}, u32[]{:S(2)}, u32[]{:S(2)}) collective-permute-start(bf16[768,128]{1,0:T(8,128)(2,1)} %get-tuple-element.14), channel_id=1, source_target_pairs={{0,57},{1,121},{2,59},{3,123},{4,61},{5,125},{6,63},{7,127},{8,49}... | collective-permute-start | bytes 589832 | tf_op jit(solution)/shard_map/ppermute | solution.py:420
  9.7 10.2 %collective-permute-start.3 = (bf16[768,128]{1,0:T(8,128)(2,1)}, bf16[768,128]{1,0:T(8,128)(2,1)S(1)}, u32[]{:S(2)}, u32[]{:S(2)}) collective-permute-start(bf16[768,128]{1,0:T(8,128)(2,1)} %get-tuple-element.13), channel_id=1, source_target_pairs={{0,56},{1,120},{2,58},{3,122},{4,60},{5,124},{6,62},{7,126},{8,48}... | collective-permute-start | bytes 589832 | tf_op jit(solution)/shard_map/ppermute | solution.py:420
  10.3 9.6 %collective-permute-start.2 = (bf16[768,128]{1,0:T(8,128)(2,1)}, bf16[768,128]{1,0:T(8,128)(2,1)S(1)}, u32[]{:S(2)}, u32[]{:S(2)}) collective-permute-start(bf16[768,128]{1,0:T(8,128)(2,1)} %get-tuple-element.12), channel_id=1, source_target_pairs={{0,1},{1,65},{2,3},{3,67},{4,5},{5,69},{6,7},{7,71},{8,9},{9,73},{... | collective-permute-start | bytes 589832 | tf_op jit(solution)/shard_map/ppermute | solution.py:420
  11.5 10.1 %collective-permute-start.1 = (bf16[768,128]{1,0:T(8,128)(2,1)}, bf16[768,128]{1,0:T(8,128)(2,1)S(1)}, u32[]{:S(2)}, u32[]{:S(2)}) collective-permute-start(bf16[768,128]{1,0:T(8,128)(2,1)} %get-tuple-element.11), channel_id=1, source_target_pairs={{0,0},{1,64},{2,2},{3,66},{4,4},{5,68},{6,6},{7,70},{8,8},{9,72},{... | collective-permute-start | bytes 589832 | tf_op jit(solution)/shard_map/ppermute | solution.py:420
  19.9 1.7 copy-start.9
  19.9 1.7 copy-start.10
  21.7 0.7 copy-start.11
  22.4 28.3 %copy-start.1 = (bf16[2048,128]{1,0:T(8,128)(2,1)}, bf16[2048,128]{1,0:T(8,128)(2,1)S(1)}, u32[]{:S(2)}) copy-start(bf16[2048,128]{1,0:T(8,128)(2,1)S(1)} %pad_maximum_fusion.refs_6_) | copy-start | bytes 1572868
  22.4 12.6 %collective-permute-start.6 = (bf16[2048,128]{1,0:T(8,128)(2,1)S(1)}, bf16[2048,128]{1,0:T(8,128)(2,1)S(1)}, u32[]{:S(2)}, u32[]{:S(2)}) collective-permute-start(bf16[2048,128]{1,0:T(8,128)(2,1)S(1)} %pad_maximum_fusion.refs_6_), channel_id=1, source_target_pairs={{0,8},{8,16},{16,24},{24,0},{32,40},{40,48},{48,56},{56,32},{64,72... | collective-permute-start | bytes 1572872 | tf_op jit(solution)/shard_map/ppermute | solution.py:430
  22.5 12.6 %collective-permute-start.8 = (bf16[2048,128]{1,0:T(8,128)(2,1)S(1)}, bf16[2048,128]{1,0:T(8,128)(2,1)S(1)}, u32[]{:S(2)}, u32[]{:S(2)}) collective-permute-start(bf16[2048,128]{1,0:T(8,128)(2,1)S(1)} %pad_maximum_fusion.refs_6_), channel_id=1, source_target_pairs={{0,24},{8,0},{16,8},{24,16},{32,56},{40,32},{48,40},{56,48},{64,88... | collective-permute-start | bytes 1572872 | tf_op jit(solution)/shard_map/ppermute | solution.py:431
  35.0 15.7 %copy-start.2 = (bf16[2048,128]{1,0:T(8,128)(2,1)}, bf16[2048,128]{1,0:T(8,128)(2,1)S(1)}, u32[]{:S(2)}) copy-start(bf16[2048,128]{1,0:T(8,128)(2,1)S(1)} %collective-permute-done.6.refs_8_) | copy-start | bytes 1572868
  35.0 8.1 %collective-permute-start.10 = (bf16[1024,128]{1,0:T(8,128)(2,1)S(1)}, bf16[1024,128]{1,0:T(8,128)(2,1)S(1)}, u32[]{:S(2)}, u32[]{:S(2)}) collective-permute-start(bf16[1024,128]{1,0:T(8,128)(2,1)S(1)} %slice.48), channel_id=1, source_target_pairs={{0,8},{8,16},{16,24},{24,0},{32,40},{40,48},{48,56},{56,32},{64,72... | collective-permute-start | bytes 786440 | tf_op jit(solution)/shard_map/ppermute | solution.py:433
  35.1 15.6 %copy-start.3 = (bf16[2048,128]{1,0:T(8,128)(2,1)}, bf16[2048,128]{1,0:T(8,128)(2,1)S(1)}, u32[]{:S(2)}) copy-start(bf16[2048,128]{1,0:T(8,128)(2,1)S(1)} %collective-permute-done.8.refs_10_) | copy-start | bytes 1572868
  35.1 8.1 %collective-permute-start.11 = (bf16[1024,128]{1,0:T(8,128)(2,1)S(1)}, bf16[1024,128]{1,0:T(8,128)(2,1)S(1)}, u32[]{:S(2)}, u32[]{:S(2)}) collective-permute-start(bf16[1024,128]{1,0:T(8,128)(2,1)S(1)} %slice.49), channel_id=1, source_target_pairs={{0,24},{8,0},{16,8},{24,16},{32,56},{40,32},{48,40},{56,48},{64,88... | collective-permute-start | bytes 786440 | tf_op jit(solution)/shard_map/ppermute | solution.py:434
  38.0 12.0 %collective-permute-start.5 = (bf16[2048,128]{1,0:T(8,128)(2,1)S(1)}, bf16[2048,128]{1,0:T(8,128)(2,1)S(1)}, u32[]{:S(2)}, u32[]{:S(2)}) collective-permute-start(bf16[2048,128]{1,0:T(8,128)(2,1)S(1)} %pad_maximum_fusion.refs_6_), channel_id=1, source_target_pairs={{0,1},{1,0},{2,3},{3,2},{4,5},{5,4},{6,7},{7,6},{8,9},{9,8},{10,11... | collective-permute-start | bytes 1572872 | tf_op jit(solution)/shard_map/ppermute | solution.py:428
  38.0 12.0 %collective-permute-start.7 = (bf16[2048,128]{1,0:T(8,128)(2,1)S(1)}, bf16[2048,128]{1,0:T(8,128)(2,1)S(1)}, u32[]{:S(2)}, u32[]{:S(2)}) collective-permute-start(bf16[2048,128]{1,0:T(8,128)(2,1)S(1)} %collective-permute-done.6.refs_8_), channel_id=1, source_target_pairs={{0,1},{1,0},{2,3},{3,2},{4,5},{5,4},{6,7},{7,6},{8,9},{9,8},{10,11... | collective-permute-start | bytes 1572872 | tf_op jit(solution)/shard_map/ppermute | solution.py:428
  38.6 11.5 %collective-permute-start.9 = (bf16[2048,128]{1,0:T(8,128)(2,1)S(1)}, bf16[2048,128]{1,0:T(8,128)(2,1)}, u32[]{:S(2)}, u32[]{:S(2)}) collective-permute-start(bf16[2048,128]{1,0:T(8,128)(2,1)S(1)} %collective-permute-done.8.refs_10_), channel_id=1, source_target_pairs={{0,1},{1,0},{2,3},{3,2},{4,5},{5,4},{6,7},{7,6},{8,9},{9,8},{10,11... | collective-permute-start | bytes 1572872 | tf_op jit(solution)/shard_map/ppermute | solution.py:428
  43.3 7.4 %copy-start.4 = (bf16[2048,128]{1,0:T(8,128)(2,1)}, bf16[2048,128]{1,0:T(8,128)(2,1)S(1)}, u32[]{:S(2)}) copy-start(bf16[2048,128]{1,0:T(8,128)(2,1)S(1)} %constant_dynamic-update-slice_fusion.refs_12_) | copy-start | bytes 1572868
  43.3 7.4 %collective-permute-start.12 = (bf16[2048,128]{1,0:T(8,128)(2,1)S(1)}, bf16[2048,128]{1,0:T(8,128)(2,1)}, u32[]{:S(2)}, u32[]{:S(2)}) collective-permute-start(bf16[2048,128]{1,0:T(8,128)(2,1)S(1)} %constant_dynamic-update-slice_fusion.refs_12_), channel_id=1, source_target_pairs={{0,1},{1,0},{2,3},{3,2},{4,5},{5,4},{6,7},{7,6},{8,9},{9,8},{10,11... | collective-permute-start | bytes 1572872 | tf_op jit(solution)/shard_map/ppermute | solution.py:428
  44.5 6.2 %copy-start.8 = (f32[256,128]{1,0:T(8,128)}, f32[256,128]{1,0:T(8,128)S(1)}, u32[]{:S(2)}) copy-start(f32[256,128]{1,0:T(8,128)S(1)} %reshape.24.refs_0_) | copy-start | bytes 393220
  44.5 5.5 %collective-permute-start = (f32[256,128]{1,0:T(8,128)S(1)}, f32[256,128]{1,0:T(8,128)S(1)}, u32[]{:S(2)}, u32[]{:S(2)}) collective-permute-start(f32[256,128]{1,0:T(8,128)S(1)} %reshape.24.refs_0_), channel_id=1, source_target_pairs={{0,1},{1,0},{2,3},{3,2},{4,5},{5,4},{6,7},{7,6},{8,9},{9,8},{10,11... | collective-permute-start | bytes 393224 | tf_op jit(solution)/shard_map/ppermute | solution.py:416
  50.0 60.2 %copy-start.13 = (s32[128,2]{0,1:T(2,128)S(1)}, s32[128,2]{0,1:T(2,128)}, u32[]{:S(2)}) copy-start(s32[128,2]{0,1:T(2,128)} %param.23) | copy-start | bytes 3076
  50.0 0.7 copy-start.12
  50.0 0.8 copy-start.6
  50.1 1.0 copy-start.7
  100.5 19.6 %all-to-all-start = ((bf16[16,64,128]{2,1,0:T(8,128)(2,1)}), bf16[16,64,128]{2,1,0:T(8,128)(2,1)S(1)}, u32[]{:S(2)}, u32[]{:S(2)}) async-start(bf16[16,64,128]{2,1,0:T(8,128)(2,1)} %attend.1), calls=%async_computation | async-start | bytes 524288 | tf_op jit(solution)/shard_map/all_to_all | solution.py:444
  120.1 0.7 copy-start.5
  168.2 5.0 %copy-start.14 = (f32[128,2]{0,1:T(2,128)S(1)}, f32[128,2]{0,1:T(2,128)}, u32[]{:S(2)}) copy-start(f32[128,2]{0,1:T(2,128)} %param.24) | copy-start | bytes 3076
  168.2 29.5 %all-to-all-start.2 = ((bf16[128,48,128]{2,1,0:T(8,128)(2,1)}), bf16[128,48,128]{2,1,0:T(8,128)(2,1)S(1)}, u32[]{:S(2)}, u32[]{:S(2)}) async-start(bf16[128,48,128]{2,1,0:T(8,128)(2,1)} %bitcast.13), calls=%async_computation.2 | async-start | bytes 3145728 | tf_op jit(solution)/shard_map/all_to_all | solution.py:467
  197.7 1.2 copy-start
